TPU v7x, 32 devices: a whole 2x2x4 slice. The times are simulated.
32 devices in a mesh: grp: 2 (over x), st: 4 (over y, core), tp: 4 (over z).
Axes of the slice: x: 2, y: 2, z: 4, core: 2. Of those that a mesh axis runs over, the one named last changes fastest.
Arguments:
- tokens: bfloat16 [4096, 2048], P(('grp', 'st')), parts along dimension 0, may hold values from -6 to 6, as said below
- store: bfloat16 [64, 128, 2048], P(('grp', 'st')), parts along dimension 0, may hold values from -6 to 6, as said below
- passage_ids: int32 [64, 4], P(('grp', 'st')), parts along dimension 0, may hold values from 0 to 31, as said below
- mix_gain: float32 [2048], replicated, may hold values from 0.1 to 1.9
- glu_value: bfloat16 [2048, 1024], P(None, 'tp'), may hold values from -0.125 to 0.125
- glu_gate: bfloat16 [2048, 1024], P(None, 'tp'), may hold values from -0.125 to 0.125
- conv_taps: bfloat16 [31, 1024], P(None, 'tp'), may hold values from -5 to 5
- channel_gain: float32 [1024], P('tp'), may hold values from 0.1 to 1.9
- mix_out: bfloat16 [1024, 2048], P('tp'), may hold values from -0.1875 to 0.1875
- query_gain: float32 [2048], replicated, may hold values from 0.1 to 1.9
- passage_gain: float32 [2048], replicated, may hold values from 0.1 to 1.9
- query_proj: bfloat16 [2048, 2048], P(None, 'tp'), may hold values from -1 to 1
- key_proj: bfloat16 [2048, 2048], P(None, 'tp'), may hold values from -1 to 1
- value_proj: bfloat16 [2048, 2048], P(None, 'tp'), may hold values from -0.125 to 0.125
- attn_out: bfloat16 [2048, 2048], P('tp'), may hold values from -0.125 to 0.125
- blend_gain: float32 [2048], replicated, may hold values from 0.5 to 3
Outputs:
- blended: bfloat16 [4096, 2048], P(('grp', 'st', 'tp')), parts along dimension 0
There are 2 independent parts, one for each index of `grp`. A program takes and returns all parts, laid end to end along the dimension named above; an argument that names none is the same for every part. Nothing has to cross between parts.
Inputs may be any that keep to these rules, and one draw needn't show every extreme that they name: `tokens`: standard normal entries clipped to the range. `store`: standard normal entries clipped to the range. `passage_ids`: passage p is held by index p // 8 of st. The 32 requests of the 8 blocks of one index of st (repeats counted) name at most 16 passages held by any one index of st, and in every draw one index of st receives exactly 16 requests from every index of st.
All inputs are finite; a program needn't handle non-finite values.
Results may differ from a plain program's by a relative error of at most 0.01575.
The roundings to bfloat16 on the way count: a program that leaves them out, or rounds other values in their place, can miss the bound.
Values may be sent and summed in bfloat16 or wider, within the bound.
A program may use at most 128 MiB of HBM per device.

v0:
```python
import functools

import jax
import jax.numpy as jnp
from jax import lax
from jax.sharding import PartitionSpec as P
from jax.experimental import pallas as pl
from jax.experimental.pallas import tpu as pltpu

CA = 1024
HD = 256
SEQ_LEN = 128


EPS = 1e-06


def rms_rows(row_data, gain_vec):
    floats = row_data.astype(jnp.float32)
    inv_scale = lax.rsqrt(jnp.mean(floats * floats, axis=-1, keepdims=True) + EPS)
    return (floats * inv_scale * gain_vec).astype(jnp.bfloat16)


def depthwise(gated_rows, conv_taps):
    span_width = conv_taps.shape[0]
    half_span = (span_width - 1) // 2
    seq_length = gated_rows.shape[1]
    padded = jnp.pad(
        gated_rows.astype(jnp.float32), ((0, 0), (half_span, span_width - 1 - half_span), (0, 0))
    )
    running = jnp.zeros(gated_rows.shape, jnp.float32)
    for tap_index in range(span_width):
        running = running + padded[:, tap_index : tap_index + seq_length] * conv_taps[
            tap_index
        ].astype(jnp.float32)
    return running


def passage_attention(queries, keys_values, head_count):
    groups, block_len, span_width = queries.shape
    head_dim = span_width // head_count
    row_count = keys_values.shape[1]
    query_heads = queries.reshape(groups, block_len, head_count, head_dim)
    key_heads = keys_values[:, :, :span_width].reshape(groups, row_count, head_count, head_dim)
    value_heads = keys_values[:, :, span_width:].reshape(groups, row_count, head_count, head_dim)
    scores = jnp.einsum(
        "gqhd,grhd->ghqr", query_heads, key_heads, preferred_element_type=jnp.float32
    ) * head_dim ** (-0.5)
    row_top = jnp.max(scores, axis=-1)
    exponent = jnp.exp(scores - row_top[..., None])
    row_sum = jnp.sum(exponent, axis=-1)
    weights = exponent.astype(jnp.bfloat16)
    outputs = jnp.einsum(
        "ghqr,grhd->gqhd", weights, value_heads, preferred_element_type=jnp.float32
    ).astype(jnp.bfloat16)
    return (outputs.reshape(groups, block_len, span_width), row_top, row_sum)


def combine(outs, tops, sums, head_count):
    batch_count, passage_count, block_len, span_width = outs.shape
    head_dim = span_width // head_count
    best_top = jnp.max(tops, axis=1, keepdims=True)
    weight = jnp.exp(tops - best_top)
    numerator = jnp.einsum(
        "bphq,bpqhd->bqhd",
        weight,
        outs.astype(jnp.float32).reshape(
            batch_count, passage_count, block_len, head_count, head_dim
        ),
    )
    denominator = jnp.sum(weight * sums, axis=1)
    result = numerator / jnp.transpose(denominator, (0, 2, 1))[..., None]
    return result.reshape(batch_count, block_len, span_width).astype(jnp.bfloat16)


def local(
    tokens,
    store,
    passage_ids,
    mix_gain,
    glu_value,
    glu_gate,
    conv_taps,
    channel_gain,
    mix_out,
    query_gain,
    passage_gain,
    query_proj,
    key_proj,
    value_proj,
    attn_out,
    blend_gain,
):
    owners = lax.axis_size("st")
    tok_rows = tokens.shape[0]
    model_width = tokens.shape[1]
    local_channels = glu_value.shape[1]
    head_width = query_proj.shape[1]
    local_heads = head_width // HD
    block_count = passage_ids.shape[0]
    per_block = passage_ids.shape[1]
    block_len = tok_rows // block_count
    requests = block_count * per_block
    capacity = 2 * requests // owners
    pass_local = store.shape[0]
    pass_rows = store.shape[1]
    flat_ids = passage_ids.reshape(requests)
    owner_of = flat_ids // pass_local
    local_of = flat_ids - owner_of * pass_local
    request_index = jnp.arange(requests)
    earlier = (owner_of[:, None] == owner_of[None, :]) & (
        request_index[None, :] < request_index[:, None]
    )
    ranking = jnp.sum(earlier.astype(jnp.int32), axis=1)
    slot_of = owner_of * capacity + ranking
    slot_ids = (
        jnp.zeros((owners * capacity,), jnp.int32)
        .at[slot_of]
        .set(local_of)
        .reshape(owners, capacity)
    )
    asked = lax.all_to_all(slot_ids, "st", split_axis=0, concat_axis=0, tiled=True)
    normed_store = rms_rows(store.reshape(pass_local * pass_rows, model_width), passage_gain)
    key_rows = jnp.dot(normed_store, key_proj, preferred_element_type=jnp.float32).astype(
        jnp.bfloat16
    )
    value_rows = jnp.dot(normed_store, value_proj, preferred_element_type=jnp.float32).astype(
        jnp.bfloat16
    )
    memory = jnp.concatenate([key_rows, value_rows], axis=1).reshape(
        pass_local, pass_rows, 2 * head_width
    )
    queries = jnp.dot(
        rms_rows(tokens, query_gain), query_proj, preferred_element_type=jnp.float32
    ).astype(jnp.bfloat16)
    query_blocks = queries.reshape(block_count, block_len, head_width)
    repeated = jnp.repeat(query_blocks, per_block, axis=0)
    served = memory[asked.reshape(owners * capacity)]
    slot_queries = (
        jnp.zeros((owners * capacity, block_len, head_width), jnp.bfloat16)
        .at[slot_of]
        .set(repeated)
    )
    visiting = lax.all_to_all(
        slot_queries.reshape(owners, capacity, block_len, head_width),
        "st",
        split_axis=0,
        concat_axis=0,
        tiled=True,
    )
    answer_out, answer_top, answer_sum = passage_attention(
        visiting.reshape(owners * capacity, block_len, head_width), served, local_heads
    )
    back_out = lax.all_to_all(
        answer_out.reshape(owners, capacity, block_len, head_width),
        "st",
        split_axis=0,
        concat_axis=0,
        tiled=True,
    )
    back_top, back_sum = (
        lax.all_to_all(
            answer_top.reshape(owners, capacity, local_heads, block_len),
            "st",
            split_axis=0,
            concat_axis=0,
            tiled=True,
        ),
        lax.all_to_all(
            answer_sum.reshape(owners, capacity, local_heads, block_len),
            "st",
            split_axis=0,
            concat_axis=0,
            tiled=True,
        ),
    )
    partial_out = back_out.reshape(owners * capacity, block_len, head_width)[slot_of]
    partial_top = back_top.reshape(owners * capacity, local_heads, block_len)[slot_of]
    partial_sum = back_sum.reshape(owners * capacity, local_heads, block_len)[slot_of]
    attended = combine(
        partial_out.reshape(block_count, per_block, block_len, head_width),
        partial_top.reshape(block_count, per_block, local_heads, block_len),
        partial_sum.reshape(block_count, per_block, local_heads, block_len),
        local_heads,
    ).reshape(tok_rows, head_width)
    mix_input = rms_rows(tokens, mix_gain)
    value_part = jnp.dot(mix_input, glu_value, preferred_element_type=jnp.float32)
    gate_part = jnp.dot(mix_input, glu_gate, preferred_element_type=jnp.float32)
    gated_rows = (value_part * jax.nn.sigmoid(gate_part)).astype(jnp.bfloat16)
    conv_rows = depthwise(gated_rows.reshape(-1, SEQ_LEN, local_channels), conv_taps).reshape(
        tok_rows, local_channels
    )
    channel_sum, channel_square = lax.psum(
        (jnp.sum(conv_rows, axis=1), jnp.sum(conv_rows * conv_rows, axis=1)), "tp"
    )
    row_mean = channel_sum / CA
    row_var = channel_square / CA - row_mean * row_mean
    activation = jax.nn.silu(
        (conv_rows - row_mean[:, None]) * lax.rsqrt(row_var + EPS)[:, None] * channel_gain
    ).astype(jnp.bfloat16)
    conv_term = jnp.dot(activation, mix_out, preferred_element_type=jnp.float32)
    attn_term = jnp.dot(attended, attn_out, preferred_element_type=jnp.float32)
    return lax.psum_scatter(
        (conv_term + blend_gain * attn_term).astype(jnp.bfloat16),
        "tp",
        scatter_dimension=0,
        tiled=True,
    )


BF = jnp.bfloat16
F32 = jnp.float32
NEG = -3e38


def mm(a, b):
    return jnp.dot(a, b, preferred_element_type=F32)


def wait_in(ref, sem):
    pltpu.make_async_copy(ref, ref, sem).wait()


def layer_kernel(
    n_st, n_tp, block_count, per_block, block_len, local_heads, seq_len, pass_rows,
    tokens_h, store_h, ids_v, mix_gain, gv_h, gg_h, taps, channel_gain, mo_h, query_gain,
    passage_gain, qw_h, kw_h, vw_h, ao_h, blend_gain,
    out_ref,
    tok, sto, gv, gg, mo, qw, kw, vw, ao, load_sem,
    ids_all, ids_s, ids_send, ids_recv, ids_sem,
    q_all, q_stage, q_send, q_recv,
    k_all, v_all, k_stage, v_stage, kv_send, kv_recv,
    gp, conv, scol, stat_all, stat_send, stat_recv, act,
    out_o, out_s, ret_o, ret_s, o_send, o_recv, s_send, s_recv,
    part, from_left, from_right, r_send, r_recv,
):
    st = lax.axis_index("st")
    tp = lax.axis_index("tp")
    core = lax.rem(st, 2)
    chip = st // 2
    n_chip = n_st // 2
    other = 1 - core
    T = tok.shape[0]
    R = sto.shape[0]
    HW = q_stage.shape[1]
    CL = act.shape[1]

    loads = []
    for n, (a, b) in enumerate(
        [(tokens_h, tok), (qw_h, qw), (store_h, sto), (kw_h, kw), (vw_h, vw), (gv_h, gv),
         (gg_h, gg), (mo_h, mo), (ao_h, ao)]
    ):
        c = pltpu.make_async_copy(a, b, load_sem.at[n])
        c.start()
        loads.append(c)

    barrier = pltpu.get_barrier_semaphore()
    for i in range(1, n_st):
        pl.semaphore_signal(barrier, inc=1, device_id={"st": lax.rem(st + i, n_st)},
                            device_id_type=pl.DeviceIdType.MESH)
    for i in range(1, n_tp):
        pl.semaphore_signal(barrier, inc=1, device_id={"tp": lax.rem(tp + i, n_tp)},
                            device_id_type=pl.DeviceIdType.MESH)

    def remote(src, dst, ssem, rsem, axis, to):
        return pltpu.make_async_remote_copy(
            src_ref=src, dst_ref=dst, send_sem=ssem, recv_sem=rsem, device_id={axis: to},
            device_id_type=pl.DeviceIdType.MESH)

    chunk_rows = T // n_tp
    table = [sorted(range(n_tp), key=lambda d: -abs(d - t)) for t in range(n_tp)]

    def chunk_at(k):
        d = jnp.int32(table[0][k])
        for t in range(1, n_tp):
            d = jnp.where(tp == t, table[t][k], d)
        return d

    chunks = [chunk_at(k) for k in range(n_tp)]

    def chunk_ds(d):
        return pl.ds(pl.multiple_of(d * chunk_rows, chunk_rows), chunk_rows)

    def peers():
        res = [(chip * 2 + other, True, 0)]
        for j in range(1, n_chip):
            c = lax.rem(chip + j, n_chip)
            res.append((c * 2 + core, False, 2 * j - 1))
            res.append((c * 2 + other, True, 2 * j))
        return res

    loads[0].wait()
    loads[1].wait()
    TC = 256
    mine = pl.ds(pl.multiple_of(core * HW, HW), HW)
    theirs = pl.ds(pl.multiple_of(other * HW, HW), HW)

    def tok_chunk(i, carry):
        rows = pl.ds(pl.multiple_of(i * TC, TC), TC)
        x = tok[rows, :].astype(F32)
        y = x * lax.rsqrt(jnp.mean(x * x, axis=-1, keepdims=True) + EPS)
        qr = (y * query_gain[...]).astype(BF)
        q_all[st, rows, :] = mm(qr, qw[:, mine]).astype(BF)
        q_stage[rows, :] = mm(qr, qw[:, theirs]).astype(BF)
        tok[rows, :] = (y * mix_gain[...]).astype(BF)
        return carry

    lax.fori_loop(0, T // TC, tok_chunk, 0)

    pl.semaphore_wait(barrier, n_st - 1 + n_tp - 1)
    for i in range(1, n_st):
        remote(ids_v, ids_all.at[st], ids_send.at[i], ids_recv.at[st], "st",
               lax.rem(st + i, n_st)).start()
    ids_own = pltpu.make_async_copy(ids_v, ids_all.at[st], ids_recv.at[st])
    ids_own.start()

    def q_copies(k):
        rows = chunk_ds(chunks[k])
        for to, stage, n in peers():
            src = q_stage.at[rows] if stage else q_all.at[st, rows]
            yield remote(src, q_all.at[st, rows], q_send.at[n, k], q_recv.at[st, k], "st", to)

    for k in range(n_tp):
        for c in q_copies(k):
            c.start()

    for n in range(2, 5):
        loads[n].wait()
    RC = 512
    n_rc = R // RC
    RP = RC // pass_rows
    pass_local = R // pass_rows
    partner = chip * 2 + other

    def store_chunk(i, carry):
        rows = pl.ds(pl.multiple_of(i * RC, RC), RC)
        x = sto[rows, :].astype(F32)
        n = (x * lax.rsqrt(jnp.mean(x * x, axis=-1, keepdims=True) + EPS) * passage_gain[...]).astype(BF)
        here, slots = pl.ds(i * RP, RP), pl.ds(core * pass_local + i * RP, RP)
        k_stage[here] = mm(n, kw[:, theirs]).astype(BF).reshape(RP, pass_rows, HW)
        v_stage[here] = mm(n, vw[:, theirs]).astype(BF).reshape(RP, pass_rows, HW)
        remote(k_stage.at[here], k_all.at[slots], kv_send.at[0, i], kv_recv.at[0, i], "st", partner).start()
        remote(v_stage.at[here], v_all.at[slots], kv_send.at[1, i], kv_recv.at[1, i], "st", partner).start()
        k_all[slots] = mm(n, kw[:, mine]).astype(BF).reshape(RP, pass_rows, HW)
        v_all[slots] = mm(n, vw[:, mine]).astype(BF).reshape(RP, pass_rows, HW)
        return carry

    lax.fori_loop(0, n_rc, store_chunk, 0)

    ids_own.wait()
    for i in range(1, n_st):
        r = lax.rem(st + i, n_st)
        remote(ids_v, ids_all.at[r], ids_send.at[i], ids_recv.at[r], "st", r).wait_recv()
    c = pltpu.make_async_copy(ids_all, ids_s, ids_sem)
    c.start()
    c.wait()

    def kv_wait(i, carry):
        here, slots = pl.ds(i * RP, RP), pl.ds(other * pass_local + i * RP, RP)
        remote(k_stage.at[here], k_all.at[slots], kv_send.at[0, i], kv_recv.at[0, i], "st", partner).wait()
        remote(v_stage.at[here], v_all.at[slots], kv_send.at[1, i], kv_recv.at[1, i], "st", partner).wait()
        return carry

    lax.fori_loop(0, n_rc, kv_wait, 0)

    heads = local_heads // 2
    HD_ = HW // heads
    per_chip = 2 * pass_local
    chunk_blocks = block_count // n_tp
    clane = lax.broadcasted_iota(jnp.int32, (chunk_rows, 128), 1)
    scale = HD_ ** (-0.5)

    def order(i):
        return lax.rem(chip + 1 + i // 2, n_chip) * 2 + lax.rem(core + 1 - i % 2, 2)

    def answer_copies(k, r):
        rows = chunk_ds(chunks[k])
        return (
            remote(out_o.at[r, rows], ret_o.at[st, rows], o_send.at[r, k], o_recv.at[st, k], "st", r),
            remote(out_s.at[r, k], ret_s.at[st, k], s_send.at[r, k], s_recv.at[st, k], "st", r),
        )

    def attend(k):
        d = chunks[k]
        rows = chunk_ds(d)

        def one(i, carry):
            r = order(i)

            @pl.when(i < n_st - 1)
            def _():
                remote(q_all.at[st, rows], q_all.at[r, rows], q_send.at[0, k], q_recv.at[r, k], "st", r).wait_recv()

            stats = jnp.zeros((chunk_rows, 128), F32)
            for h in range(heads):
                cols = slice(h * HD_, (h + 1) * HD_)
                tops, dens = [], []
                for u in range(chunk_blocks):
                    b = d * chunk_blocks + u
                    brow = pl.ds(pl.multiple_of(b * block_len, block_len), block_len)
                    q = q_all[r, brow, cols]
                    ks, vs, bias = [], [], []
                    for j in range(per_block):
                        p = ids_s[r, b, j] - chip * per_chip
                        spread_p = jnp.full((1, pass_rows), p, jnp.int32)
                        valid = jnp.logical_and(spread_p >= 0, spread_p < per_chip)
                        bias.append(jnp.where(valid, 0.0, NEG))
                        slot = jnp.clip(p, 0, per_chip - 1)
                        ks.append(k_all[slot][:, cols])
                        vs.append(v_all[slot][:, cols])
                    s = lax.dot_general(q, jnp.concatenate(ks, axis=0), (((1,), (1,)), ((), ())),
                                        preferred_element_type=F32)
                    s = s * scale + jnp.concatenate(bias, axis=1)
                    top = jnp.maximum(jnp.max(s, axis=1, keepdims=True), NEG / 2)
                    e = jnp.exp(s - top)
                    dens.append(jnp.sum(e, axis=1, keepdims=True))
                    tops.append(top)
                    out_o[r, brow, cols] = mm(e.astype(BF), jnp.concatenate(vs, axis=0)).astype(BF)
                stats = jnp.where(clane == 2 * h, jnp.concatenate(tops, axis=0), stats)
                stats = jnp.where(clane == 2 * h + 1, jnp.concatenate(dens, axis=0), stats)
            out_s[r, k] = jnp.transpose(stats)[:8]

            @pl.when(i < n_st - 1)
            def _():
                for c in answer_copies(k, r):
                    c.start()

            return carry

        lax.fori_loop(0, n_st, one, 0)

    attend(0)

    loads[5].wait()
    loads[6].wait()
    per_seq = seq_len
    pad = (gp.shape[1] - per_seq) // 2
    gp[:, :pad] = jnp.zeros((gp.shape[0], pad, CL), F32)
    gp[:, pad + per_seq:] = jnp.zeros((gp.shape[0], pad, CL), F32)

    def glu_chunk(i, carry):
        mr = tok[pl.ds(pl.multiple_of(i * TC, TC), TC), :]
        gated = (mm(mr, gv[...]) * jax.nn.sigmoid(mm(mr, gg[...]))).astype(BF).astype(F32)
        for u in range(TC // per_seq):
            gp[i * (TC // per_seq) + u, pad:pad + per_seq, :] = gated[u * per_seq:(u + 1) * per_seq]
        return carry

    lax.fori_loop(0, T // TC, glu_chunk, 0)
    tap_values = taps[...].astype(F32)
    n_tap = taps.shape[0]
    lead = pad - (n_tap - 1) // 2
    CC = 64
    per = per_seq // CC
    lane = lax.broadcasted_iota(jnp.int32, (CC, 128), 1)

    def conv_chunk(i, carry):
        seq = i // per
        base = pl.multiple_of(lax.rem(i, per) * CC, CC)
        win = gp[seq, pl.ds(base, CC + 2 * pad), :]
        acc = None
        for res in range(8):
            group = None
            for k in range(n_tap):
                if (lead + k) % 8 == res:
                    at = lead + k - res
                    term = win[at:at + CC + (8 if res else 0)] * tap_values[k:k + 1]
                    group = term if group is None else group + term
            if group is not None:
                group = group[res:res + CC]
                acc = group if acc is None else acc + group
        rows = pl.ds(pl.multiple_of(i * CC, CC), CC)
        conv[rows, :] = acc
        s = jnp.sum(acc, axis=1, keepdims=True)
        ss = jnp.sum(acc * acc, axis=1, keepdims=True)
        scol[rows, :] = jnp.where(lane == 0, s, jnp.where(lane == 1, ss, 0.0))
        return carry

    lax.fori_loop(0, T // CC, conv_chunk, 0)
    stat_all[tp] = jnp.transpose(scol[...])[:8]
    for i in range(1, n_tp):
        remote(stat_all.at[tp], stat_all.at[tp], stat_send.at[i], stat_recv.at[tp], "tp",
               lax.rem(tp + i, n_tp)).start()

    attend(1)

    total = stat_all[tp]
    for i in range(1, n_tp):
        r = lax.rem(tp + i, n_tp)
        remote(stat_all.at[tp], stat_all.at[r], stat_send.at[i], stat_recv.at[r], "tp", r).wait_recv()
        total = total + stat_all[r]
    ca = CL * n_tp
    mean = total / ca
    spread = jnp.transpose(jnp.concatenate([mean, jnp.zeros((120, T), F32)], axis=0))
    row_mean = spread[:, 0:1]
    inv = lax.rsqrt(spread[:, 1:2] - row_mean * row_mean + EPS)
    a = (conv[...] - row_mean) * inv * channel_gain[...]
    act[...] = (a / (1.0 + jnp.exp(-a))).astype(BF)
    loads[7].wait()
    loads[8].wait()

    SUB = 4
    SR = chunk_rows // SUB

    def hop(k, u, ahead, buf, way):
        d = chunks[k]
        prow = pl.ds(pl.multiple_of(d * chunk_rows + u * SR, SR), SR)
        brow = pl.ds(u * SR, SR)
        to = jnp.clip(tp + ahead, 0, n_tp - 1)
        return prow, brow, remote(part.at[prow], buf.at[d, brow], r_send.at[way, d, u],
                                  r_recv.at[way, d, u], "tp", to)

    ways = ((1, from_left, 0), (-1, from_right, 1))

    def goes(k, way):
        return tp < chunks[k] if way == 0 else tp > chunks[k]

    def at_end(way):
        return tp == 0 if way == 0 else tp == n_tp - 1

    def finish(k):
        rows = chunk_ds(chunks[k])
        for i in range(n_st - 1):
            r = order(i)
            remote(out_o.at[r, rows], ret_o.at[r, rows], o_send.at[r, k], o_recv.at[r, k], "st", r).wait_recv()
            remote(out_s.at[r, k], ret_s.at[r, k], s_send.at[r, k], s_recv.at[r, k], "st", r).wait_recv()
        ret_o[st, rows, :] = out_o[st, rows, :]
        ret_s[st, k] = out_s[st, k]
        stats = jnp.transpose(jnp.concatenate(
            [ret_s[c, k] for c in range(n_st)] + [jnp.zeros((128 - 8 * n_st, chunk_rows), F32)], axis=0))
        pieces = []
        for g in range(2):
            for h in range(heads):
                cols = slice(h * HD_, (h + 1) * HD_)
                at = [8 * (c * 2 + g) + 2 * h for c in range(n_chip)]
                best = functools.reduce(jnp.maximum, [stats[:, x:x + 1] for x in at])
                num, den = 0.0, 0.0
                for c in range(n_chip):
                    w = jnp.exp(stats[:, at[c]:at[c] + 1] - best)
                    num = num + w * ret_o[c * 2 + g, rows, cols].astype(F32)
                    den = den + w * stats[:, at[c] + 1:at[c] + 2]
                pieces.append((num / den).astype(BF))
        attended = jnp.concatenate(pieces, axis=1)
        act_rows = act[rows, :]
        NC = 512
        for i in range(part.shape[1] // NC):
            cols = slice(i * NC, (i + 1) * NC)
            value = mm(act_rows, mo[:, cols]) + blend_gain[:, cols] * mm(attended, ao[:, cols])
            part[rows, cols] = value.astype(BF)
        if k < n_tp - 1:
            for ahead, buf, way in ways:
                @pl.when(jnp.logical_and(goes(k, way), at_end(way)))
                def _(ahead=ahead, buf=buf, way=way):
                    for u in range(SUB):
                        hop(k, u, ahead, buf, way)[2].start()

    def forward(k, u):
        for ahead, buf, way in ways:
            @pl.when(jnp.logical_and(goes(k, way), jnp.logical_not(at_end(way))))
            def _(ahead=ahead, buf=buf, way=way):
                prow, brow, copy = hop(k, u, ahead, buf, way)
                copy.wait_recv()
                part[prow, :] = (part[prow, :].astype(F32) + buf[chunks[k], brow, :].astype(F32)).astype(BF)
                copy.start()

    forwarded = 0
    for k in range(n_tp):
        finish(k)
        if k + 2 < n_tp:
            attend(k + 2)
        elif k < n_tp - 1:
            for u in range(SUB):
                forward(k - 2, u)
            forwarded = k - 1
    for u in range(SUB):
        for k in range(forwarded, n_tp - 1):
            forward(k, u)

    for u in range(SUB):
        prow = pl.ds(pl.multiple_of(tp * chunk_rows + u * SR, SR), SR)
        brow = pl.ds(u * SR, SR)

        for ahead, buf, way in ways:
            @pl.when(jnp.logical_not(at_end(way)))
            def _(buf=buf, way=way, ahead=ahead):
                to = jnp.clip(tp - ahead, 0, n_tp - 1)
                remote(part.at[prow], buf.at[tp, brow], r_send.at[way, tp, u], r_recv.at[way, tp, u], "tp",
                       to).wait_recv()

            @pl.when(at_end(way))
            def _(buf=buf):
                buf[tp, brow, :] = jnp.zeros((SR, part.shape[1]), BF)

        out_ref[brow, :] = (
            part[prow, :].astype(F32) + from_left[tp, brow, :].astype(F32) + from_right[tp, brow, :].astype(F32)
        ).astype(BF)

    for i in range(1, n_st):
        r = lax.rem(st + i, n_st)
        remote(ids_v, ids_all.at[st], ids_send.at[i], ids_recv.at[st], "st", r).wait_send()
    for k in range(n_tp):
        for c in q_copies(k):
            c.wait_send()
        for i in range(n_st - 1):
            for c in answer_copies(k, order(i)):
                c.wait_send()
    for i in range(1, n_tp):
        remote(stat_all.at[tp], stat_all.at[tp], stat_send.at[i], stat_recv.at[tp], "tp",
               lax.rem(tp + i, n_tp)).wait_send()
    for k in range(n_tp - 1):
        for ahead, buf, way in ways:
            @pl.when(goes(k, way))
            def _(ahead=ahead, buf=buf, way=way):
                for u in range(SUB):
                    hop(k, u, ahead, buf, way)[2].wait_send()


def fused_local(
    tokens, store, passage_ids, mix_gain, glu_value, glu_gate, conv_taps, channel_gain, mix_out,
    query_gain, passage_gain, query_proj, key_proj, value_proj, attn_out, blend_gain,
):
    n_st = lax.axis_size("st")
    n_tp = lax.axis_size("tp")
    T, D = tokens.shape
    P_, PR, _ = store.shape
    R = P_ * PR
    W = query_proj.shape[1]
    HW = W // 2
    CL = glu_value.shape[1]
    nb, per_block = passage_ids.shape
    ids = jnp.pad(passage_ids, ((0, 0), (0, 128 - per_block)))
    pad = 8 * pl.cdiv((conv_taps.shape[0] - 1) // 2, 8)
    DMA = pltpu.SemaphoreType.DMA
    V = pltpu.VMEM
    SUB = 4
    kern = functools.partial(layer_kernel, n_st, n_tp, nb, per_block, T // nb, W // HD, SEQ_LEN, PR)
    hbm = pl.BlockSpec(memory_space=pl.ANY)
    vm = pl.BlockSpec(memory_space=pltpu.VMEM)
    return pl.pallas_call(
        kern,
        out_shape=jax.ShapeDtypeStruct((T // n_tp, D), BF),
        in_specs=[hbm, hbm, vm, vm, hbm, hbm, vm, vm, hbm, vm, vm, hbm, hbm, hbm, hbm, vm],
        out_specs=vm,
        scratch_shapes=[
            V((T, D), BF), V((R, D), BF), V((D, CL), BF), V((D, CL), BF), V((CL, D), BF),
            V((D, W), BF), V((D, W), BF), V((D, W), BF), V((W, D), BF), DMA((9,)),
            V((n_st, nb, 128), jnp.int32), pltpu.SMEM((n_st, nb, 128), jnp.int32),
            DMA((n_st,)), DMA((n_st,)), DMA,
            V((n_st, T, HW), BF), V((T, HW), BF), DMA((n_st - 1, n_tp)), DMA((n_st, n_tp)),
            V((2 * P_, PR, HW), BF), V((2 * P_, PR, HW), BF), V((P_, PR, HW), BF), V((P_, PR, HW), BF),
            DMA((2, R // 512)), DMA((2, R // 512)),
            V((T // SEQ_LEN, SEQ_LEN + 2 * pad, CL), F32), V((T, CL), F32), V((T, 128), F32),
            V((n_tp, 8, T), F32), DMA((n_tp,)), DMA((n_tp,)), V((T, CL), BF),
            V((n_st, T, HW), BF), V((n_st, n_tp, 8, T // n_tp), F32), V((n_st, T, HW), BF),
            V((n_st, n_tp, 8, T // n_tp), F32),
            DMA((n_st, n_tp)), DMA((n_st, n_tp)), DMA((n_st, n_tp)), DMA((n_st, n_tp)),
            V((T, D), BF), V((n_tp, T // n_tp, D), BF), V((n_tp, T // n_tp, D), BF),
            DMA((2, n_tp, SUB)), DMA((2, n_tp, SUB)),
        ],
        compiler_params=pltpu.CompilerParams(
            collective_id=0, has_side_effects=True, vmem_limit_bytes=60 * 1024 * 1024),
        name="layer",
    )(
        tokens, store.reshape(R, D), ids, mix_gain.reshape(1, D), glu_value, glu_gate, conv_taps,
        channel_gain.reshape(1, CL), mix_out, query_gain.reshape(1, D), passage_gain.reshape(1, D),
        query_proj, key_proj, value_proj, attn_out, blend_gain.reshape(1, D),
    )


def solution(mesh):
    in_specs = (
        P(("grp", "st"), None),
        P(("grp", "st"), None, None),
        P(("grp", "st"), None),
        P(),
        P(None, "tp"),
        P(None, "tp"),
        P(None, "tp"),
        P("tp"),
        P("tp", None),
        P(),
        P(),
        P(None, "tp"),
        P(None, "tp"),
        P(None, "tp"),
        P("tp", None),
        P(),
    )
    out_specs = P(("grp", "st", "tp"), None)
    def body(*args):
        even = args[11].shape[1] // HD % 2 == 0 and mesh.shape["st"] % 2 == 0
        even = even and args[2].shape[0] % mesh.shape["tp"] == 0 and mesh.shape["st"] <= 16
        return (fused_local if even else local)(*args)

    return jax.shard_map(body, mesh=mesh, in_specs=in_specs, out_specs=out_specs, check_vma=False)
```

profile of v0, /device:TPU:0, one launch (start us, length us, event | category | flops | bytes accessed | tf_op | source)
XLA Modules:
  0.0 66.6 jit_solution(13359502207954797918)
XLA Ops:
  0.0 0.8 %copy.17 = s32[8,4]{1,0:T(8,128)S(1)} copy(s32[8,4]{0,1:T(4,128)} %param.18) | data formatting | bytes 256 | tf_op args[2]
  0.8 0.6 pad.4.ids_v
  1.4 63.4 %layer.1 = bf16[128,2048]{1,0:T(8,128)(2,1)} custom-call(bf16[512,2048]{1,0:T(8,128)(2,1)} %tokens_h.1, bf16[1024,2048]{1,0:T(8,128)(2,1)} %bitcast.6, s32[8,128]{1,0:T(8,128)} %pad.4.ids_v, f32[1,2048]{1,0:T(1,128)} %bitcast.7, bf16[2048,256]{1,0:T(8,128)(2,1)} %gv_h.1, bf16[2048,256]{1,0:T(8,128)(2,1)} %gg_h.1, bf16[31,256]{1,0:T(8,128)(2,1)} %taps.1, ...), custom_call_target="tpu_custom_call" | custom-call | tf_op jit(solution)/shard_map/layer/pallas_call | solution.py:638
  64.7 1.9 %copy.19 = bf16[128,2048]{1,0:T(8,128)(2,1)} copy(bf16[128,2048]{1,0:T(8,128)(2,1)} %layer.1) | data formatting | bytes 1048576
where the time goes:
time: 66.9 us; the launch traced here: 66.6 us
  Pallas kernels  63.4 us (95%)
  local copies, waits for them, and re-layouts  3.24 us (5%)
    pallas_call x1, Pallas kernels, fused_local(): pl.pallas_call(kern, out_shape=jax.ShapeDtypeStruct((T // n_tp, D), BF),...  63.4 us
    unnamed x2, local copies, waits for them, and re-layouts  2.64 us

commit v1 on v0

--- a/solution.py
+++ b/solution.py
@@ -211,6 +211,7 @@
 BF = jnp.bfloat16
 F32 = jnp.float32
 NEG = -3e38
+VMEM_MIB = 60
 
 
 def mm(a, b):
@@ -223,10 +224,11 @@
 
 def layer_kernel(
     n_st, n_tp, block_count, per_block, block_len, local_heads, seq_len, pass_rows,
-    tokens_h, store_h, ids_v, mix_gain, gv_h, gg_h, taps, channel_gain, mo_h, query_gain,
-    passage_gain, qw_h, kw_h, vw_h, ao_h, blend_gain,
+    tokens_h, store_h, ids_h, mix_h, gv_h, gg_h, taps_h, channel_h, mo_h, query_h,
+    passage_h, qw_h, kw_h, vw_h, ao_h, blend_h,
     out_ref,
     tok, sto, gv, gg, mo, qw, kw, vw, ao, load_sem,
+    ids_v, mix_gain, taps, channel_gain, query_gain, passage_gain, blend_gain, small_sem,
     ids_all, ids_s, ids_send, ids_recv, ids_sem,
     q_all, q_stage, q_send, q_recv,
     k_all, v_all, k_stage, v_stage, kv_send, kv_recv,
@@ -245,6 +247,14 @@
     HW = q_stage.shape[1]
     CL = act.shape[1]
 
+    smalls = []
+    for n, (a, b) in enumerate(
+        [(query_h, query_gain), (mix_h, mix_gain), (ids_h, ids_v), (passage_h, passage_gain), (taps_h, taps),
+         (channel_h, channel_gain), (blend_h, blend_gain)]
+    ):
+        c = pltpu.make_async_copy(a, b, small_sem.at[n])
+        c.start()
+        smalls.append(c)
     loads = []
     for n, (a, b) in enumerate(
         [(tokens_h, tok), (qw_h, qw), (store_h, sto), (kw_h, kw), (vw_h, vw), (gv_h, gv),
@@ -289,6 +299,8 @@
             res.append((c * 2 + other, True, 2 * j))
         return res
 
+    for c in smalls:
+        c.wait()
     loads[0].wait()
     loads[1].wait()
     TC = 256
@@ -384,50 +396,61 @@
         d = chunks[k]
         rows = chunk_ds(d)
 
-        def one(i, carry):
-            r = order(i)
-
-            @pl.when(i < n_st - 1)
-            def _():
-                remote(q_all.at[st, rows], q_all.at[r, rows], q_send.at[0, k], q_recv.at[r, k], "st", r).wait_recv()
-
+        def pair(g, carry):
+            rs = [order(2 * g), order(2 * g + 1)]
+            for e, r in enumerate(rs):
+                @pl.when(jnp.logical_or(e == 0, g < n_chip - 1))
+                def _(r=r):
+                    remote(q_all.at[st, rows], q_all.at[r, rows], q_send.at[0, k], q_recv.at[r, k], "st", r).wait_recv()
+
+            units = [(e, h, u) for e in range(2) for h in range(heads) for u in range(chunk_blocks)]
+            place, values, scores = {}, {}, {}
+            for e, h, u in units:
+                r = rs[e]
+                cols = slice(h * HD_, (h + 1) * HD_)
+                b = d * chunk_blocks + u
+                brow = pl.ds(pl.multiple_of(b * block_len, block_len), block_len)
+                ks, vs, bias = [], [], []
+                for j in range(per_block):
+                    p = ids_s[r, j, b] - chip * per_chip
+                    spread_p = jnp.full((1, pass_rows), p, jnp.int32)
+                    valid = jnp.logical_and(spread_p >= 0, spread_p < per_chip)
+                    bias.append(jnp.where(valid, 0.0, NEG))
+                    slot = jnp.clip(p, 0, per_chip - 1)
+                    ks.append(k_all[slot][:, cols])
+                    vs.append(v_all[slot][:, cols])
+                s = lax.dot_general(q_all[r, brow, cols], jnp.concatenate(ks, axis=0), (((1,), (1,)), ((), ())),
+                                    preferred_element_type=F32)
+                scores[e, h, u] = s * scale + jnp.concatenate(bias, axis=1)
+                values[e, h, u] = jnp.concatenate(vs, axis=0)
+                place[e, h, u] = (r, brow, cols)
+            tops = {n: jnp.maximum(jnp.max(scores[n], axis=1, keepdims=True), NEG / 2) for n in units}
+            weights, dens = {}, {}
+            for n in units:
+                exponent = jnp.exp(scores[n] - tops[n])
+                dens[n] = jnp.sum(exponent, axis=1, keepdims=True)
+                weights[n] = exponent.astype(BF)
+            for n in units:
+                r, brow, cols = place[n]
+                out_o[r, brow, cols] = mm(weights[n], values[n]).astype(BF)
             stats = jnp.zeros((chunk_rows, 128), F32)
-            for h in range(heads):
-                cols = slice(h * HD_, (h + 1) * HD_)
-                tops, dens = [], []
-                for u in range(chunk_blocks):
-                    b = d * chunk_blocks + u
-                    brow = pl.ds(pl.multiple_of(b * block_len, block_len), block_len)
-                    q = q_all[r, brow, cols]
-                    ks, vs, bias = [], [], []
-                    for j in range(per_block):
-                        p = ids_s[r, b, j] - chip * per_chip
-                        spread_p = jnp.full((1, pass_rows), p, jnp.int32)
-                        valid = jnp.logical_and(spread_p >= 0, spread_p < per_chip)
-                        bias.append(jnp.where(valid, 0.0, NEG))
-                        slot = jnp.clip(p, 0, per_chip - 1)
-                        ks.append(k_all[slot][:, cols])
-                        vs.append(v_all[slot][:, cols])
-                    s = lax.dot_general(q, jnp.concatenate(ks, axis=0), (((1,), (1,)), ((), ())),
-                                        preferred_element_type=F32)
-                    s = s * scale + jnp.concatenate(bias, axis=1)
-                    top = jnp.maximum(jnp.max(s, axis=1, keepdims=True), NEG / 2)
-                    e = jnp.exp(s - top)
-                    dens.append(jnp.sum(e, axis=1, keepdims=True))
-                    tops.append(top)
-                    out_o[r, brow, cols] = mm(e.astype(BF), jnp.concatenate(vs, axis=0)).astype(BF)
-                stats = jnp.where(clane == 2 * h, jnp.concatenate(tops, axis=0), stats)
-                stats = jnp.where(clane == 2 * h + 1, jnp.concatenate(dens, axis=0), stats)
-            out_s[r, k] = jnp.transpose(stats)[:8]
-
-            @pl.when(i < n_st - 1)
-            def _():
-                for c in answer_copies(k, r):
-                    c.start()
+            for e in range(2):
+                for h in range(heads):
+                    for at, parts in ((2 * h, tops), (2 * h + 1, dens)):
+                        column = jnp.concatenate([parts[e, h, u] for u in range(chunk_blocks)], axis=0)
+                        stats = jnp.where(clane == 8 * e + at, column, stats)
+            turned = jnp.transpose(stats)
+            for e, r in enumerate(rs):
+                out_s[r, k] = turned[8 * e:8 * e + 8]
+
+                @pl.when(jnp.logical_or(e == 0, g < n_chip - 1))
+                def _(r=r):
+                    for c in answer_copies(k, r):
+                        c.start()
 
             return carry
 
-        lax.fori_loop(0, n_st, one, 0)
+        lax.fori_loop(0, n_chip, pair, 0)
 
     attend(0)
 
@@ -627,7 +650,6 @@
     HW = W // 2
     CL = glu_value.shape[1]
     nb, per_block = passage_ids.shape
-    ids = jnp.pad(passage_ids, ((0, 0), (0, 128 - per_block)))
     pad = 8 * pl.cdiv((conv_taps.shape[0] - 1) // 2, 8)
     DMA = pltpu.SemaphoreType.DMA
     V = pltpu.VMEM
@@ -637,13 +659,15 @@
     vm = pl.BlockSpec(memory_space=pltpu.VMEM)
     return pl.pallas_call(
         kern,
-        out_shape=jax.ShapeDtypeStruct((T // n_tp, D), BF),
-        in_specs=[hbm, hbm, vm, vm, hbm, hbm, vm, vm, hbm, vm, vm, hbm, hbm, hbm, hbm, vm],
+        out_shape=pltpu.VMEM((T // n_tp, D), BF),
+        in_specs=[hbm] * 16,
         out_specs=vm,
         scratch_shapes=[
             V((T, D), BF), V((R, D), BF), V((D, CL), BF), V((D, CL), BF), V((CL, D), BF),
             V((D, W), BF), V((D, W), BF), V((D, W), BF), V((W, D), BF), DMA((9,)),
-            V((n_st, nb, 128), jnp.int32), pltpu.SMEM((n_st, nb, 128), jnp.int32),
+            V((per_block, nb), jnp.int32), V((1, D), F32), V(conv_taps.shape, BF), V((1, CL), F32), V((1, D), F32),
+            V((1, D), F32), V((1, D), F32), DMA((7,)),
+            V((n_st, per_block, nb), jnp.int32), pltpu.SMEM((n_st, per_block, nb), jnp.int32),
             DMA((n_st,)), DMA((n_st,)), DMA,
             V((n_st, T, HW), BF), V((T, HW), BF), DMA((n_st - 1, n_tp)), DMA((n_st, n_tp)),
             V((2 * P_, PR, HW), BF), V((2 * P_, PR, HW), BF), V((P_, PR, HW), BF), V((P_, PR, HW), BF),
@@ -657,10 +681,10 @@
             DMA((2, n_tp, SUB)), DMA((2, n_tp, SUB)),
         ],
         compiler_params=pltpu.CompilerParams(
-            collective_id=0, has_side_effects=True, vmem_limit_bytes=60 * 1024 * 1024),
+            collective_id=0, has_side_effects=True, vmem_limit_bytes=VMEM_MIB * 1024 * 1024),
         name="layer",
     )(
-        tokens, store.reshape(R, D), ids, mix_gain.reshape(1, D), glu_value, glu_gate, conv_taps,
+        tokens, store.reshape(R, D), passage_ids.T, mix_gain.reshape(1, D), glu_value, glu_gate, conv_taps,
         channel_gain.reshape(1, CL), mix_out, query_gain.reshape(1, D), passage_gain.reshape(1, D),
         query_proj, key_proj, value_proj, attn_out, blend_gain.reshape(1, D),
     )

time: 66.9 us -> 64.4 us (0.963)
  local copies, waits for them, and re-layouts: 3.24 us -> 0.8 us
    unnamed x2 -> x1, local copies, waits for them, and re-layouts: 2.64 us -> 0.8 us
where the time goes in v1:
time: 64.4 us; the launch traced here: 64.2 us
  Pallas kernels  63.4 us (98%)
  local copies, waits for them, and re-layouts  0.8 us (1%)
    pallas_call x1, Pallas kernels, fused_local(): pl.pallas_call(kern, out_shape=pltpu.VMEM((T // n_tp, D), BF), in_specs=[...  63.4 us

profile of v1, /device:TPU:0, one launch (start us, length us, event | category | flops | bytes accessed | tf_op | source)
XLA Modules:
  0.0 64.2 jit_solution(9820478090643723827)
XLA Ops:
  0.0 63.4 %layer.1 = bf16[128,2048]{1,0:T(8,128)(2,1)S(1)} custom-call(bf16[512,2048]{1,0:T(8,128)(2,1)} %tokens_h.1, bf16[1024,2048]{1,0:T(8,128)(2,1)} %bitcast.7, s32[4,8]{1,0:T(4,128)} %bitcast.12, f32[1,2048]{1,0:T(1,128)} %bitcast.8, bf16[2048,256]{1,0:T(8,128)(2,1)} %gv_h.1, bf16[2048,256]{1,0:T(8,128)(2,1)} %gg_h.1, bf16[31,256]{1,0:T(8,128)(2,1)} %taps_h.1, ...), custom_call_target="tpu_custom_call" | custom-call | tf_op jit(solution)/shard_map/layer/pallas_call | solution.py:660
  63.4 0.8 %copy.18 = bf16[128,2048]{1,0:T(8,128)(2,1)} copy(bf16[128,2048]{1,0:T(8,128)(2,1)S(1)} %layer.1) | data formatting | bytes 1048576

commit v2 on v1

--- a/solution.py
+++ b/solution.py
@@ -212,6 +212,7 @@
 F32 = jnp.float32
 NEG = -3e38
 VMEM_MIB = 60
+PRIO = 1
 
 
 def mm(a, b):
@@ -247,22 +248,16 @@
     HW = q_stage.shape[1]
     CL = act.shape[1]
 
-    smalls = []
-    for n, (a, b) in enumerate(
-        [(query_h, query_gain), (mix_h, mix_gain), (ids_h, ids_v), (passage_h, passage_gain), (taps_h, taps),
-         (channel_h, channel_gain), (blend_h, blend_gain)]
-    ):
-        c = pltpu.make_async_copy(a, b, small_sem.at[n])
+    small_pairs = [(query_h, query_gain), (mix_h, mix_gain), (ids_h, ids_v), (passage_h, passage_gain),
+                   (taps_h, taps), (channel_h, channel_gain), (blend_h, blend_gain)]
+    big_pairs = [(tokens_h, tok), (qw_h, qw), (store_h, sto), (kw_h, kw), (vw_h, vw), (gv_h, gv), (gg_h, gg),
+                 (mo_h, mo), (ao_h, ao)]
+    smalls = [pltpu.make_async_copy(a, b, small_sem.at[n]) for n, (a, b) in enumerate(small_pairs)]
+    loads = [pltpu.make_async_copy(a, b, load_sem.at[n]) for n, (a, b) in enumerate(big_pairs)]
+    for c in smalls[:3] + loads[:2]:
         c.start()
-        smalls.append(c)
-    loads = []
-    for n, (a, b) in enumerate(
-        [(tokens_h, tok), (qw_h, qw), (store_h, sto), (kw_h, kw), (vw_h, vw), (gv_h, gv),
-         (gg_h, gg), (mo_h, mo), (ao_h, ao)]
-    ):
-        c = pltpu.make_async_copy(a, b, load_sem.at[n])
-        c.start()
-        loads.append(c)
+    for c in loads[2:5] + smalls[3:] + loads[5:]:
+        c.start(priority=PRIO)
 
     barrier = pltpu.get_barrier_semaphore()
     for i in range(1, n_st):
@@ -299,8 +294,8 @@
             res.append((c * 2 + other, True, 2 * j))
         return res
 
-    for c in smalls:
-        c.wait()
+    smalls[0].wait()
+    smalls[1].wait()
     loads[0].wait()
     loads[1].wait()
     TC = 256
@@ -320,6 +315,7 @@
     lax.fori_loop(0, T // TC, tok_chunk, 0)
 
     pl.semaphore_wait(barrier, n_st - 1 + n_tp - 1)
+    smalls[2].wait()
     for i in range(1, n_st):
         remote(ids_v, ids_all.at[st], ids_send.at[i], ids_recv.at[st], "st",
                lax.rem(st + i, n_st)).start()
@@ -336,6 +332,7 @@
         for c in q_copies(k):
             c.start()
 
+    smalls[3].wait()
     for n in range(2, 5):
         loads[n].wait()
     RC = 512
@@ -454,6 +451,7 @@
 
     attend(0)
 
+    smalls[4].wait()
     loads[5].wait()
     loads[6].wait()
     per_seq = seq_len
@@ -506,6 +504,8 @@
 
     attend(1)
 
+    smalls[5].wait()
+    smalls[6].wait()
     total = stat_all[tp]
     for i in range(1, n_tp):
         r = lax.rem(tp + i, n_tp)

time: 64.4 us -> 61.7 us (0.958)
  Pallas kernels: 63.4 us -> 60.8 us
    pallas_call x1, Pallas kernels: 63.4 us -> 60.8 us  [fused_local(): pl.pallas_call(kern, out_shape=pltpu.VMEM((T // n_tp, D), BF), in_specs=[...]
where the time goes in v2:
time: 61.7 us; the launch traced here: 61.6 us
  Pallas kernels  60.8 us (99%)
  local copies, waits for them, and re-layouts  0.8 us (1%)
    pallas_call x1, Pallas kernels, fused_local(): pl.pallas_call(kern, out_shape=pltpu.VMEM((T // n_tp, D), BF), in_specs=[...  60.8 us

profile of v2, /device:TPU:0, one launch (start us, length us, event | category | flops | bytes accessed | tf_op | source)
XLA Modules:
  0.0 61.6 jit_solution(5201995771705922044)
XLA Ops:
  0.0 60.8 %layer.1 = bf16[128,2048]{1,0:T(8,128)(2,1)S(1)} custom-call(bf16[512,2048]{1,0:T(8,128)(2,1)} %tokens_h.1, bf16[1024,2048]{1,0:T(8,128)(2,1)} %bitcast.7, s32[4,8]{1,0:T(4,128)} %bitcast.12, f32[1,2048]{1,0:T(1,128)} %bitcast.8, bf16[2048,256]{1,0:T(8,128)(2,1)} %gv_h.1, bf16[2048,256]{1,0:T(8,128)(2,1)} %gg_h.1, bf16[31,256]{1,0:T(8,128)(2,1)} %taps_h.1, ...), custom_call_target="tpu_custom_call" | custom-call | tf_op jit(solution)/shard_map/layer/pallas_call | solution.py:660
  60.8 0.8 %copy.18 = bf16[128,2048]{1,0:T(8,128)(2,1)} copy(bf16[128,2048]{1,0:T(8,128)(2,1)S(1)} %layer.1) | data formatting | bytes 1048576

commit v3 on v2

v3 whole, which is shorter than its diff:
```python
import functools

import jax
import jax.numpy as jnp
from jax import lax
from jax.sharding import PartitionSpec as P
from jax.experimental import pallas as pl
from jax.experimental.pallas import tpu as pltpu

CA = 1024
HD = 256
SEQ_LEN = 128


EPS = 1e-06


def rms_rows(row_data, gain_vec):
    floats = row_data.astype(jnp.float32)
    inv_scale = lax.rsqrt(jnp.mean(floats * floats, axis=-1, keepdims=True) + EPS)
    return (floats * inv_scale * gain_vec).astype(jnp.bfloat16)


def depthwise(gated_rows, conv_taps):
    span_width = conv_taps.shape[0]
    half_span = (span_width - 1) // 2
    seq_length = gated_rows.shape[1]
    padded = jnp.pad(
        gated_rows.astype(jnp.float32), ((0, 0), (half_span, span_width - 1 - half_span), (0, 0))
    )
    running = jnp.zeros(gated_rows.shape, jnp.float32)
    for tap_index in range(span_width):
        running = running + padded[:, tap_index : tap_index + seq_length] * conv_taps[
            tap_index
        ].astype(jnp.float32)
    return running


def passage_attention(queries, keys_values, head_count):
    groups, block_len, span_width = queries.shape
    head_dim = span_width // head_count
    row_count = keys_values.shape[1]
    query_heads = queries.reshape(groups, block_len, head_count, head_dim)
    key_heads = keys_values[:, :, :span_width].reshape(groups, row_count, head_count, head_dim)
    value_heads = keys_values[:, :, span_width:].reshape(groups, row_count, head_count, head_dim)
    scores = jnp.einsum(
        "gqhd,grhd->ghqr", query_heads, key_heads, preferred_element_type=jnp.float32
    ) * head_dim ** (-0.5)
    row_top = jnp.max(scores, axis=-1)
    exponent = jnp.exp(scores - row_top[..., None])
    row_sum = jnp.sum(exponent, axis=-1)
    weights = exponent.astype(jnp.bfloat16)
    outputs = jnp.einsum(
        "ghqr,grhd->gqhd", weights, value_heads, preferred_element_type=jnp.float32
    ).astype(jnp.bfloat16)
    return (outputs.reshape(groups, block_len, span_width), row_top, row_sum)


def combine(outs, tops, sums, head_count):
    batch_count, passage_count, block_len, span_width = outs.shape
    head_dim = span_width // head_count
    best_top = jnp.max(tops, axis=1, keepdims=True)
    weight = jnp.exp(tops - best_top)
    numerator = jnp.einsum(
        "bphq,bpqhd->bqhd",
        weight,
        outs.astype(jnp.float32).reshape(
            batch_count, passage_count, block_len, head_count, head_dim
        ),
    )
    denominator = jnp.sum(weight * sums, axis=1)
    result = numerator / jnp.transpose(denominator, (0, 2, 1))[..., None]
    return result.reshape(batch_count, block_len, span_width).astype(jnp.bfloat16)


def local(
    tokens,
    store,
    passage_ids,
    mix_gain,
    glu_value,
    glu_gate,
    conv_taps,
    channel_gain,
    mix_out,
    query_gain,
    passage_gain,
    query_proj,
    key_proj,
    value_proj,
    attn_out,
    blend_gain,
):
    owners = lax.axis_size("st")
    tok_rows = tokens.shape[0]
    model_width = tokens.shape[1]
    local_channels = glu_value.shape[1]
    head_width = query_proj.shape[1]
    local_heads = head_width // HD
    block_count = passage_ids.shape[0]
    per_block = passage_ids.shape[1]
    block_len = tok_rows // block_count
    requests = block_count * per_block
    capacity = 2 * requests // owners
    pass_local = store.shape[0]
    pass_rows = store.shape[1]
    flat_ids = passage_ids.reshape(requests)
    owner_of = flat_ids // pass_local
    local_of = flat_ids - owner_of * pass_local
    request_index = jnp.arange(requests)
    earlier = (owner_of[:, None] == owner_of[None, :]) & (
        request_index[None, :] < request_index[:, None]
    )
    ranking = jnp.sum(earlier.astype(jnp.int32), axis=1)
    slot_of = owner_of * capacity + ranking
    slot_ids = (
        jnp.zeros((owners * capacity,), jnp.int32)
        .at[slot_of]
        .set(local_of)
        .reshape(owners, capacity)
    )
    asked = lax.all_to_all(slot_ids, "st", split_axis=0, concat_axis=0, tiled=True)
    normed_store = rms_rows(store.reshape(pass_local * pass_rows, model_width), passage_gain)
    key_rows = jnp.dot(normed_store, key_proj, preferred_element_type=jnp.float32).astype(
        jnp.bfloat16
    )
    value_rows = jnp.dot(normed_store, value_proj, preferred_element_type=jnp.float32).astype(
        jnp.bfloat16
    )
    memory = jnp.concatenate([key_rows, value_rows], axis=1).reshape(
        pass_local, pass_rows, 2 * head_width
    )
    queries = jnp.dot(
        rms_rows(tokens, query_gain), query_proj, preferred_element_type=jnp.float32
    ).astype(jnp.bfloat16)
    query_blocks = queries.reshape(block_count, block_len, head_width)
    repeated = jnp.repeat(query_blocks, per_block, axis=0)
    served = memory[asked.reshape(owners * capacity)]
    slot_queries = (
        jnp.zeros((owners * capacity, block_len, head_width), jnp.bfloat16)
        .at[slot_of]
        .set(repeated)
    )
    visiting = lax.all_to_all(
        slot_queries.reshape(owners, capacity, block_len, head_width),
        "st",
        split_axis=0,
        concat_axis=0,
        tiled=True,
    )
    answer_out, answer_top, answer_sum = passage_attention(
        visiting.reshape(owners * capacity, block_len, head_width), served, local_heads
    )
    back_out = lax.all_to_all(
        answer_out.reshape(owners, capacity, block_len, head_width),
        "st",
        split_axis=0,
        concat_axis=0,
        tiled=True,
    )
    back_top, back_sum = (
        lax.all_to_all(
            answer_top.reshape(owners, capacity, local_heads, block_len),
            "st",
            split_axis=0,
            concat_axis=0,
            tiled=True,
        ),
        lax.all_to_all(
            answer_sum.reshape(owners, capacity, local_heads, block_len),
            "st",
            split_axis=0,
            concat_axis=0,
            tiled=True,
        ),
    )
    partial_out = back_out.reshape(owners * capacity, block_len, head_width)[slot_of]
    partial_top = back_top.reshape(owners * capacity, local_heads, block_len)[slot_of]
    partial_sum = back_sum.reshape(owners * capacity, local_heads, block_len)[slot_of]
    attended = combine(
        partial_out.reshape(block_count, per_block, block_len, head_width),
        partial_top.reshape(block_count, per_block, local_heads, block_len),
        partial_sum.reshape(block_count, per_block, local_heads, block_len),
        local_heads,
    ).reshape(tok_rows, head_width)
    mix_input = rms_rows(tokens, mix_gain)
    value_part = jnp.dot(mix_input, glu_value, preferred_element_type=jnp.float32)
    gate_part = jnp.dot(mix_input, glu_gate, preferred_element_type=jnp.float32)
    gated_rows = (value_part * jax.nn.sigmoid(gate_part)).astype(jnp.bfloat16)
    conv_rows = depthwise(gated_rows.reshape(-1, SEQ_LEN, local_channels), conv_taps).reshape(
        tok_rows, local_channels
    )
    channel_sum, channel_square = lax.psum(
        (jnp.sum(conv_rows, axis=1), jnp.sum(conv_rows * conv_rows, axis=1)), "tp"
    )
    row_mean = channel_sum / CA
    row_var = channel_square / CA - row_mean * row_mean
    activation = jax.nn.silu(
        (conv_rows - row_mean[:, None]) * lax.rsqrt(row_var + EPS)[:, None] * channel_gain
    ).astype(jnp.bfloat16)
    conv_term = jnp.dot(activation, mix_out, preferred_element_type=jnp.float32)
    attn_term = jnp.dot(attended, attn_out, preferred_element_type=jnp.float32)
    return lax.psum_scatter(
        (conv_term + blend_gain * attn_term).astype(jnp.bfloat16),
        "tp",
        scatter_dimension=0,
        tiled=True,
    )


BF = jnp.bfloat16
F32 = jnp.float32
NEG = -3e38
VMEM_MIB = 60
PRIO = 1
BEFORE = 3
RC = 512
SUB = 8
EARLY = 5


def mm(a, b):
    return jnp.dot(a, b, preferred_element_type=F32)


def wait_in(ref, sem):
    pltpu.make_async_copy(ref, ref, sem).wait()


def layer_kernel(
    n_st, n_tp, block_count, per_block, block_len, local_heads, seq_len, pass_rows,
    tokens_h, store_h, ids_h, mix_h, gv_h, gg_h, taps_h, channel_h, mo_h, query_h,
    passage_h, qw_h, kw_h, vw_h, ao_h, blend_h,
    out_ref,
    tok, sto, gv, gg, mo, qw, kw, vw, ao, load_sem,
    ids_v, mix_gain, taps, channel_gain, query_gain, passage_gain, blend_gain, small_sem,
    ids_all, ids_s, ids_send, ids_recv, ids_sem,
    q_all, q_stage, q_send, q_recv,
    k_all, v_all, k_stage, v_stage, kv_send, kv_recv,
    gp, conv, scol, stat_all, stat_send, stat_recv, act,
    out_o, out_s, ret_o, ret_s, o_send, o_recv, s_send, s_recv,
    part, inbox, r_send, r_recv,
    att, mate_act, mate_att, a_send, a_recv, mate_part, mo2, ao2, w_send, near_recv, far_recv, pass_recv,
):
    st = lax.axis_index("st")
    tp = lax.axis_index("tp")
    grp = lax.axis_index("grp")
    outer = jnp.logical_or(tp == 0, tp == n_tp - 1)
    inner = jnp.logical_not(outer)
    mate = tp + 1 - 2 * lax.rem(tp, 2)
    across = n_tp - 1 - tp
    core = lax.rem(st, 2)
    chip = st // 2
    n_chip = n_st // 2
    other = 1 - core
    T = tok.shape[0]
    R = sto.shape[0]
    HW = q_stage.shape[1]
    CL = act.shape[1]

    small_pairs = [(query_h, query_gain), (mix_h, mix_gain), (ids_h, ids_v), (passage_h, passage_gain),
                   (taps_h, taps), (channel_h, channel_gain), (blend_h, blend_gain)]
    big_pairs = [(tokens_h, tok), (qw_h, qw), (gv_h, gv), (gg_h, gg), (store_h, sto), (kw_h, kw), (vw_h, vw),
                 (mo_h, mo), (ao_h, ao)]
    smalls = [pltpu.make_async_copy(a, b, small_sem.at[n]) for n, (a, b) in enumerate(small_pairs)]
    loads = [pltpu.make_async_copy(a, b, load_sem.at[n]) for n, (a, b) in enumerate(big_pairs)]
    for c in smalls[:3] + loads[:2]:
        c.start()
    for c in loads[2:4] + smalls[3:] + loads[4:]:
        c.start(priority=PRIO)

    barrier = pltpu.get_barrier_semaphore()
    for i in range(1, n_st):
        pl.semaphore_signal(barrier, inc=1, device_id={"st": lax.rem(st + i, n_st)},
                            device_id_type=pl.DeviceIdType.MESH)
    for i in range(1, n_tp):
        pl.semaphore_signal(barrier, inc=1, device_id={"tp": lax.rem(tp + i, n_tp)},
                            device_id_type=pl.DeviceIdType.MESH)

    def remote(src, dst, ssem, rsem, axis, to):
        return pltpu.make_async_remote_copy(
            src_ref=src, dst_ref=dst, send_sem=ssem, recv_sem=rsem, device_id={axis: to},
            device_id_type=pl.DeviceIdType.MESH)

    pl.semaphore_signal(barrier, inc=1, device_id={"grp": 1 - grp}, device_id_type=pl.DeviceIdType.MESH)

    def drain(ref, sem):
        pltpu.make_async_copy(ref, ref, sem).wait()

    chunk_rows = T // n_tp
    table = [[3, 2, 1, 0], [3, 2, 0, 1], [0, 1, 3, 2], [0, 1, 2, 3]]

    def chunk_at(k):
        d = jnp.int32(table[0][k])
        for t in range(1, n_tp):
            d = jnp.where(tp == t, table[t][k], d)
        return d

    chunks = [chunk_at(k) for k in range(n_tp)]

    def chunk_ds(d):
        return pl.ds(pl.multiple_of(d * chunk_rows, chunk_rows), chunk_rows)

    def peers():
        res = [(chip * 2 + other, True, 0)]
        for j in range(1, n_chip):
            c = lax.rem(chip + j, n_chip)
            res.append((c * 2 + core, False, 2 * j - 1))
            res.append((c * 2 + other, True, 2 * j))
        return res

    partner = chip * 2 + other
    PR_ = 32
    n_ao, n_mo = HW * 2 // 4 // PR_, CL // 4 // PR_
    n_piece = n_ao + n_mo

    def weight_copy(route, p, g, c):
        src, dst, at, size = (ao_h, ao2, p, HW * 2 // 4) if p < n_ao else (mo_h, mo2, p - n_ao, CL // 4)
        rows = pl.ds(pl.multiple_of((2 * g + c) * size + at * PR_, PR_), PR_)
        axis, to = (("tp", mate), ("st", partner), ("grp", 1 - grp), ("st", partner))[route]
        arrival = (near_recv.at[p], pass_recv.at[0], far_recv.at[p], pass_recv.at[1])[route]
        return remote((dst if route else src).at[rows], dst.at[rows], w_send.at[route], arrival, axis, to)

    quarter = mo2.at[0:n_piece * PR_]

    def relay_near(*pieces):
        @pl.when(inner)
        def _():
            for p in pieces:
                weight_copy(0, p, grp, core).wait_recv()
                weight_copy(2, p, grp, core).start()
                weight_copy(1, p, grp, core).start()

    def relay_far(*pieces):
        @pl.when(inner)
        def _():
            for p in pieces:
                weight_copy(2, p, 1 - grp, core).wait_recv()
                weight_copy(3, p, 1 - grp, core).start()

    def weights_out(*pieces):
        @pl.when(outer)
        def _():
            for p in pieces:
                weight_copy(0, p, grp, core).start()

    pl.semaphore_wait(barrier, n_st - 1 + n_tp - 1 + 1)
    weights_out(*range(BEFORE))
    smalls[0].wait()
    smalls[1].wait()
    loads[0].wait()
    loads[1].wait()
    TC = 256
    mine = pl.ds(pl.multiple_of(core * HW, HW), HW)
    theirs = pl.ds(pl.multiple_of(other * HW, HW), HW)

    def tok_chunk(i, carry):
        rows = pl.ds(pl.multiple_of(i * TC, TC), TC)
        x = tok[rows, :].astype(F32)
        y = x * lax.rsqrt(jnp.mean(x * x, axis=-1, keepdims=True) + EPS)
        qr = (y * query_gain[...]).astype(BF)
        q_all[st, rows, :] = mm(qr, qw[:, mine]).astype(BF)
        q_stage[rows, :] = mm(qr, qw[:, theirs]).astype(BF)
        tok[rows, :] = (y * mix_gain[...]).astype(BF)
        return carry

    lax.fori_loop(0, T // TC, tok_chunk, 0)

    smalls[2].wait()
    for i in range(1, n_st):
        remote(ids_v, ids_all.at[st], ids_send, ids_recv, "st", lax.rem(st + i, n_st)).start()
    pltpu.make_async_copy(ids_v, ids_all.at[st], ids_recv).start()

    def q_copies(k):
        rows = chunk_ds(chunks[k])
        for to, stage, n in peers():
            src = q_stage.at[rows] if stage else q_all.at[st, rows]
            yield remote(src, q_all.at[st, rows], q_send, q_recv.at[k], "st", to)

    for k in range(n_tp):
        for c in q_copies(k):
            c.start()

    smalls[4].wait()
    loads[2].wait()
    loads[3].wait()
    per_seq = seq_len
    pad = (gp.shape[1] - per_seq) // 2
    gp[:, :pad] = jnp.zeros((gp.shape[0], pad, CL), F32)
    gp[:, pad + per_seq:] = jnp.zeros((gp.shape[0], pad, CL), F32)

    tap_values = taps[...].astype(F32)
    n_tap = taps.shape[0]
    lead = pad - (n_tap - 1) // 2
    CC = 64
    per = per_seq // CC
    lane = lax.broadcasted_iota(jnp.int32, (CC, 128), 1)

    def conv_chunk(i, carry):
        seq = i // per
        base = pl.multiple_of(lax.rem(i, per) * CC, CC)
        win = gp[seq, pl.ds(base, CC + 2 * pad), :]
        acc = None
        for res in range(8):
            group = None
            for k in range(n_tap):
                if (lead + k) % 8 == res:
                    at = lead + k - res
                    term = win[at:at + CC + (8 if res else 0)] * tap_values[k:k + 1]
                    group = term if group is None else group + term
            if group is not None:
                group = group[res:res + CC]
                acc = group if acc is None else acc + group
        rows = pl.ds(pl.multiple_of(i * CC, CC), CC)
        conv[rows, :] = acc
        s = jnp.sum(acc, axis=1, keepdims=True)
        ss = jnp.sum(acc * acc, axis=1, keepdims=True)
        scol[rows, :] = jnp.where(lane == 0, s, jnp.where(lane == 1, ss, 0.0))
        return carry

    pairs = ((0, n_tp - 1), (1, n_tp - 2))

    def glu_rows(c):
        at = c * chunk_rows
        mr = tok[at:at + chunk_rows, :]
        gated = (mm(mr, gv[...]) * jax.nn.sigmoid(mm(mr, gg[...]))).astype(BF).astype(F32)
        for u in range(chunk_rows // per_seq):
            gp[at // per_seq + u, pad:pad + per_seq, :] = gated[u * per_seq:(u + 1) * per_seq]

    def stat_copy(n, i):
        r = lax.rem(tp + i, n_tp)
        return remote(stat_all.at[tp, n], stat_all.at[tp, n], stat_send, stat_recv.at[n], "tp", r)

    def conv_pair(n):
        for c in pairs[n]:
            glu_rows(c)
        for c in pairs[n]:
            lax.fori_loop(c * chunk_rows // CC, (c + 1) * chunk_rows // CC, conv_chunk, 0)
        stat_all[tp, n] = jnp.transpose(jnp.concatenate(
            [scol[c * chunk_rows:(c + 1) * chunk_rows, :] for c in pairs[n]], axis=0))[:8]
        for i in range(1, n_tp):
            stat_copy(n, i).start()

    def act_pair(n):
        drain(stat_all.at[0:n_tp - 1, n], stat_recv.at[n])
        total = stat_all[tp, n]
        for i in range(1, n_tp):
            total = total + stat_all[lax.rem(tp + i, n_tp), n]
        mean = total / (CL * n_tp)
        spread = jnp.transpose(jnp.concatenate([mean, jnp.zeros((120, 2 * chunk_rows), F32)], axis=0))
        row_mean = spread[:, 0:1]
        inv = lax.rsqrt(spread[:, 1:2] - row_mean * row_mean + EPS)
        for j, c in enumerate(pairs[n]):
            rows, cut = slice(c * chunk_rows, (c + 1) * chunk_rows), slice(j * chunk_rows, (j + 1) * chunk_rows)
            a = (conv[rows, :] - row_mean[cut]) * inv[cut] * channel_gain[...]
            act[rows, :] = (a / (1.0 + jnp.exp(-a))).astype(BF)

    conv_pair(0)
    weights_out(*range(BEFORE, n_piece))


    drain(ids_all, ids_recv)
    ids_in = pltpu.make_async_copy(ids_all, ids_s, ids_sem)
    ids_in.start()
    smalls[3].wait()
    for n in range(4, 7):
        loads[n].wait()
    n_rc = R // RC
    RP = RC // pass_rows
    pass_local = R // pass_rows

    def norm_rows(i, part, parts):
        rows = slice(i * RC + part * RC // parts, i * RC + (part + 1) * RC // parts)
        x = sto[rows, :].astype(F32)
        y = x * lax.rsqrt(jnp.mean(x * x, axis=-1, keepdims=True) + EPS) * passage_gain[...]
        sto[rows, :] = y.astype(BF)

    for i in range(n_rc):
        norm_rows(i, 0, 1)
        here, slots = pl.ds(i * RP, RP), pl.ds(core * pass_local + i * RP, RP)
        def project(dst, at, weight, cols):
            dst[at] = mm(sto[i * RC:(i + 1) * RC, :], weight[:, cols]).astype(BF).reshape(RP, pass_rows, HW)

        project(k_stage, here, kw, theirs)
        project(v_stage, here, vw, theirs)
        remote(k_stage.at[here], k_all.at[slots], kv_send, kv_recv.at[0], "st", partner).start()
        remote(v_stage.at[here], v_all.at[slots], kv_send, kv_recv.at[1], "st", partner).start()
        relay_near(i)
        project(k_all, slots, kw, mine)
        project(v_all, slots, vw, mine)

    ids_in.wait()
    drain(k_stage, kv_recv.at[0])
    drain(v_stage, kv_recv.at[1])

    heads = local_heads // 2
    HD_ = HW // heads
    per_chip = 2 * pass_local
    chunk_blocks = block_count // n_tp
    clane = lax.broadcasted_iota(jnp.int32, (chunk_rows, 128), 1)
    scale = HD_ ** (-0.5)

    def order(i):
        return lax.rem(chip + 1 + i // 2, n_chip) * 2 + lax.rem(core + 1 - i % 2, 2)

    def answer_copies(k, r):
        rows = chunk_ds(chunks[k])
        return (
            remote(out_o.at[r, rows], ret_o.at[st, rows], o_send, o_recv.at[k], "st", r),
            remote(out_s.at[r, k], ret_s.at[st, k], s_send, s_recv.at[k], "st", r),
        )

    def attend(k):
        d = chunks[k]
        rows = chunk_ds(d)

        rs = [order(i) for i in range(n_st)]
        drain(q_all.at[0:n_st - 1, rows], q_recv.at[k])
        units = [(e, h, u) for e in range(n_st) for h in range(heads) for u in range(chunk_blocks)]
        place, values, scores, tops, dens, weights = {}, {}, {}, {}, {}, {}
        for e, h, u in units:
            r = rs[e]
            cols = slice(h * HD_, (h + 1) * HD_)
            b = d * chunk_blocks + u
            brow = pl.ds(pl.multiple_of(b * block_len, block_len), block_len)
            ks, vs, bias = [], [], []
            for j in range(per_block):
                p = ids_s[r, j, b] - chip * per_chip
                spread_p = jnp.full((1, pass_rows), p, jnp.int32)
                valid = jnp.logical_and(spread_p >= 0, spread_p < per_chip)
                bias.append(jnp.where(valid, 0.0, NEG))
                slot = jnp.clip(p, 0, per_chip - 1)
                ks.append(k_all[slot][:, cols])
                vs.append(functools.partial(lambda slot, cols: v_all[slot][:, cols], slot, cols))
            s = lax.dot_general(q_all[r, brow, cols], jnp.concatenate(ks, axis=0), (((1,), (1,)), ((), ())),
                                preferred_element_type=F32)
            scores[e, h, u] = s * scale + jnp.concatenate(bias, axis=1)
            values[e, h, u] = vs
            place[e, h, u] = (r, brow, cols)
        for e0 in range(0, n_st, 2):
            batch = [n for n in units if n[0] in (e0, e0 + 1)]
            for n in batch:
                tops[n] = jnp.maximum(jnp.max(scores[n], axis=1, keepdims=True), NEG / 2)
            for n in batch:
                exponent = jnp.exp(scores[n] - tops[n])
                dens[n] = jnp.sum(exponent, axis=1, keepdims=True)
                weights[n] = exponent.astype(BF)
            for n in batch:
                r, brow, cols = place[n]
                out_o[r, brow, cols] = mm(weights[n], jnp.concatenate([v() for v in values[n]], axis=0)).astype(BF)
            stats = jnp.zeros((chunk_rows, 128), F32)
            for e in range(2):
                for h in range(heads):
                    for at, parts in ((2 * h, tops), (2 * h + 1, dens)):
                        column = jnp.concatenate([parts[e0 + e, h, u] for u in range(chunk_blocks)], axis=0)
                        stats = jnp.where(clane == 8 * e + at, column, stats)
            turned = jnp.transpose(stats)
            for e in range(2):
                r = rs[e0 + e]
                out_s[r, k] = turned[8 * e:8 * e + 8]
                if e0 + e < n_st - 1:
                    for c in answer_copies(k, r):
                        c.start()

    attend(0)
    relay_near(2)
    conv_pair(1)
    relay_near(3)
    relay_far(0)
    attend(1)
    relay_far(1)
    attend(2)
    relay_near(4)
    relay_far(2)
    smalls[5].wait()
    smalls[6].wait()
    act_pair(0)
    loads[7].wait()
    loads[8].wait()

    SR = chunk_rows // SUB
    AH = chunk_rows // 2
    NC = 512

    def piece(lane, u):
        d = chunks[(0, 0, 1, 2)[lane]]
        rows = pl.ds(pl.multiple_of(d * chunk_rows + u * SR, SR), SR)
        slot = (0, 1, 2, 0)[lane]
        to = (mate, across, across, mate)[lane]
        box = inbox.at[slot, pl.ds(u * SR, SR)]
        return rows, slot, remote(part.at[rows], box, r_send, r_recv.at[slot, u], "tp", to)

    def rows_copies(k, half):
        rows = pl.ds(pl.multiple_of(chunks[k] * chunk_rows + half * AH, AH), AH)
        cut = pl.ds(half * AH, AH)
        return (
            remote(act.at[rows], mate_act.at[k - 1, cut], a_send.at[0], a_recv.at[0, k - 1, half], "tp", mate),
            remote(att.at[k, cut], mate_att.at[k - 1, cut], a_send.at[1], a_recv.at[1, k - 1, half], "tp", mate),
        )

    def combine(k):
        rows = chunk_ds(chunks[k])
        drain(ret_o.at[0:n_st - 1, rows], o_recv.at[k])
        drain(ret_s.at[0:n_st - 1, k], s_recv.at[k])
        ret_s[st, k] = out_s[st, k]
        stats = jnp.transpose(jnp.concatenate(
            [ret_s[c, k] for c in range(n_st)] + [jnp.zeros((128 - 8 * n_st, chunk_rows), F32)], axis=0))
        ret_o[st, rows, :] = out_o[st, rows, :]
        for g in range(2):
            for h in range(heads):
                cols = slice(h * HD_, (h + 1) * HD_)
                at = [8 * (c * 2 + g) + 2 * h for c in range(n_chip)]
                best = functools.reduce(jnp.maximum, [stats[:, x:x + 1] for x in at])
                num, den = 0.0, 0.0
                for c in range(n_chip):
                    w = jnp.exp(stats[:, at[c]:at[c] + 1] - best)
                    num = num + w * ret_o[c * 2 + g, rows, cols].astype(F32)
                    den = den + w * stats[:, at[c] + 1:at[c] + 2]
                att[k, :, (g * heads + h) * HD_:(g * heads + h + 1) * HD_] = (num / den).astype(BF)

    def own_partial(k):
        rows = chunk_ds(chunks[k])
        for i in range(part.shape[1] // NC):
            cols = slice(i * NC, (i + 1) * NC)
            part[rows, cols] = (mm(act[rows, :], mo[:, cols]) + blend_gain[:, cols] * mm(att[k], ao[:, cols])).astype(BF)

    def mate_rows(slot, half, cols):
        cut = slice(half * AH, (half + 1) * AH)
        return (mm(mate_act[slot, cut], mo2[:, cols])
                + blend_gain[:, cols] * mm(mate_att[slot, cut], ao2[:, cols])).astype(BF)

    def wait_rows(k, half):
        for c in rows_copies(k, half):
            c.wait_recv()

    def onward(lane_in, lane_out, *pieces):
        for u in pieces:
            slot = (0, 1, 2, 0)[lane_in]
            piece(lane_in, u)[2].wait_recv()
            rows, _, copy = piece(lane_out, u)
            part[rows, :] = (part[rows, :].astype(F32) + inbox[slot, pl.ds(u * SR, SR), :].astype(F32)).astype(BF)
            copy.start()

    combine(0)
    own_partial(0)

    @pl.when(outer)
    def _():
        for u in range(EARLY):
            piece(0, u)[2].start()

    relay_near(5)
    relay_far(3)
    act_pair(1)
    attend(3)
    combine(1)

    @pl.when(outer)
    def _():
        for half in range(2):
            for c in rows_copies(1, half):
                c.start()
        for u in range(EARLY, SUB):
            piece(0, u)[2].start()

    @pl.when(inner)
    def _():
        onward(0, 1, 0)
        own_partial(1)
        onward(0, 1, 1)

    combine(2)

    @pl.when(outer)
    def _():
        for half in range(2):
            for c in rows_copies(2, half):
                c.start()

    relay_far(4, 5)

    @pl.when(inner)
    def _():
        onward(0, 1, *range(2, EARLY))
        own_partial(2)

    combine(3)
    own_partial(3)

    @pl.when(inner)
    def _():
        for n in range(2):
            drain(quarter, pass_recv.at[n])
        for half in range(2):
            wait_rows(1, half)
            rows = pl.ds(pl.multiple_of(chunks[1] * chunk_rows + half * AH, AH), AH)
            for i in range(part.shape[1] // NC):
                cols = slice(i * NC, (i + 1) * NC)
                part[rows, cols] = (part[rows, cols].astype(F32) + mate_rows(0, half, cols).astype(F32)).astype(BF)
            for u in range(half * SUB // 2, (half + 1) * SUB // 2):
                piece(2, u)[2].start()
            if half == 0:
                onward(0, 1, *range(EARLY, SUB))
        onward(1, 3, *range(EARLY))
        for half in range(2):
            wait_rows(2, half)
            for i in range(part.shape[1] // NC):
                cols = slice(i * NC, (i + 1) * NC)
                mate_part[half * AH:(half + 1) * AH, cols] = mate_rows(1, half, cols)
        onward(1, 3, *range(EARLY, SUB))
        for u in range(SUB):
            rows = pl.ds(pl.multiple_of(tp * chunk_rows + u * SR, SR), SR)
            cut = pl.ds(u * SR, SR)
            piece(2, u)[2].wait_recv()
            out_ref[cut, :] = (part[rows, :].astype(F32) + mate_part[cut, :].astype(F32)
                               + inbox[2, cut, :].astype(F32)).astype(BF)

    @pl.when(outer)
    def _():
        for u in range(SUB):
            rows = pl.ds(pl.multiple_of(tp * chunk_rows + u * SR, SR), SR)
            cut = pl.ds(u * SR, SR)
            piece(3, u)[2].wait_recv()
            out_ref[cut, :] = (part[rows, :].astype(F32) + inbox[0, cut, :].astype(F32)).astype(BF)

    @pl.when(outer)
    def _():
        drain(quarter, w_send.at[0])
        drain(part.at[0:chunk_rows], r_send)
        drain(act.at[0:2 * chunk_rows], a_send.at[0])
        drain(att.at[0:2], a_send.at[1])

    @pl.when(inner)
    def _():
        for route in (1, 2, 3):
            drain(quarter, w_send.at[route])
        drain(part.at[0:3 * chunk_rows], r_send)

    drain(ids_all.at[0:n_st - 1], ids_send)
    drain(q_all.at[0:n_st - 1], q_send)
    drain(k_all, kv_send)
    drain(stat_all.at[0:n_tp - 1], stat_send)
    drain(out_o.at[0:n_st - 1], o_send)
    drain(out_s.at[0:n_st - 1], s_send)


def fused_local(
    tokens, store, passage_ids, mix_gain, glu_value, glu_gate, conv_taps, channel_gain, mix_out,
    query_gain, passage_gain, query_proj, key_proj, value_proj, attn_out, blend_gain,
):
    n_st = lax.axis_size("st")
    n_tp = lax.axis_size("tp")
    T, D = tokens.shape
    P_, PR, _ = store.shape
    R = P_ * PR
    W = query_proj.shape[1]
    HW = W // 2
    CL = glu_value.shape[1]
    nb, per_block = passage_ids.shape
    pad = 8 * pl.cdiv((conv_taps.shape[0] - 1) // 2, 8)
    DMA = pltpu.SemaphoreType.DMA
    V = pltpu.VMEM
    kern = functools.partial(layer_kernel, n_st, n_tp, nb, per_block, T // nb, W // HD, SEQ_LEN, PR)
    hbm = pl.BlockSpec(memory_space=pl.ANY)
    vm = pl.BlockSpec(memory_space=pltpu.VMEM)
    return pl.pallas_call(
        kern,
        out_shape=pltpu.VMEM((T // n_tp, D), BF),
        in_specs=[hbm] * 16,
        out_specs=vm,
        scratch_shapes=[
            V((T, D), BF), V((R, D), BF), V((D, CL), BF), V((D, CL), BF), V((CL, D), BF),
            V((D, W), BF), V((D, W), BF), V((D, W), BF), V((W, D), BF), DMA((9,)),
            V((per_block, nb), jnp.int32), V((1, D), F32), V(conv_taps.shape, BF), V((1, CL), F32), V((1, D), F32),
            V((1, D), F32), V((1, D), F32), DMA((7,)),
            V((n_st, per_block, nb), jnp.int32), pltpu.SMEM((n_st, per_block, nb), jnp.int32),
            DMA, DMA, DMA,
            V((n_st, T, HW), BF), V((T, HW), BF), DMA, DMA((n_tp,)),
            V((2 * P_, PR, HW), BF), V((2 * P_, PR, HW), BF), V((P_, PR, HW), BF), V((P_, PR, HW), BF),
            DMA, DMA((2,)),
            V((T // SEQ_LEN, SEQ_LEN + 2 * pad, CL), F32), V((T, CL), F32), V((T, 128), F32),
            V((n_tp, 2, 8, 2 * T // n_tp), F32), DMA, DMA((2,)), V((T, CL), BF),
            V((n_st, T, HW), BF), V((n_st, n_tp, 8, T // n_tp), F32), V((n_st, T, HW), BF),
            V((n_st, n_tp, 8, T // n_tp), F32),
            DMA, DMA((n_tp,)), DMA, DMA((n_tp,)),
            V((T, D), BF), V((3, T // n_tp, D), BF), DMA, DMA((3, SUB)),
            V((n_tp, T // n_tp, W), BF), V((2, T // n_tp, CL), BF), V((2, T // n_tp, W), BF),
            DMA((2,)), DMA((2, 2, 2)), V((T // n_tp, D), BF), V((CL, D), BF), V((W, D), BF),
            DMA((4,)), DMA(((W + CL) // 128,)), DMA(((W + CL) // 128,)), DMA((2,)),
        ],
        compiler_params=pltpu.CompilerParams(
            collective_id=0, has_side_effects=True, vmem_limit_bytes=VMEM_MIB * 1024 * 1024),
        name="layer",
    )(
        tokens, store.reshape(R, D), passage_ids.T, mix_gain.reshape(1, D), glu_value, glu_gate, conv_taps,
        channel_gain.reshape(1, CL), mix_out, query_gain.reshape(1, D), passage_gain.reshape(1, D),
        query_proj, key_proj, value_proj, attn_out, blend_gain.reshape(1, D),
    )


def solution(mesh):
    in_specs = (
        P(("grp", "st"), None),
        P(("grp", "st"), None, None),
        P(("grp", "st"), None),
        P(),
        P(None, "tp"),
        P(None, "tp"),
        P(None, "tp"),
        P("tp"),
        P("tp", None),
        P(),
        P(),
        P(None, "tp"),
        P(None, "tp"),
        P(None, "tp"),
        P("tp", None),
        P(),
    )
    out_specs = P(("grp", "st", "tp"), None)
    def body(*args):
        even = args[11].shape[1] // HD % 2 == 0 and mesh.shape["st"] % 2 == 0
        even = even and args[2].shape[0] % mesh.shape["tp"] == 0 and mesh.shape["st"] <= 16
        even = even and mesh.shape["tp"] == 4 and mesh.shape["grp"] == 2 and mesh.shape["st"] == 4
        even = even and args[0].shape[0] % (SEQ_LEN * mesh.shape["tp"]) == 0
        return (fused_local if even else local)(*args)

    return jax.shard_map(body, mesh=mesh, in_specs=in_specs, out_specs=out_specs, check_vma=False)
```

time: 61.7 us -> 58.3 us (0.945)
  Pallas kernels: 60.8 us -> 57.4 us
    pallas_call x1, Pallas kernels: 60.8 us -> 57.4 us  [fused_local(): pl.pallas_call(kern, out_shape=pltpu.VMEM((T // n_tp, D), BF), in_specs=[...]
where the time goes in v3:
time: 58.3 us; the launch traced here: 58.2 us
  Pallas kernels  57.4 us (98%)
  local copies, waits for them, and re-layouts  0.8 us (1%)
    pallas_call x1, Pallas kernels, fused_local(): pl.pallas_call(kern, out_shape=pltpu.VMEM((T // n_tp, D), BF), in_specs=[...  57.4 us

profile of v3, /device:TPU:0, one launch (start us, length us, event | category | flops | bytes accessed | tf_op | source)
XLA Modules:
  0.0 58.2 jit_solution(3983532736298782816)
XLA Ops:
  0.0 57.4 %layer.1 = bf16[128,2048]{1,0:T(8,128)(2,1)S(1)} custom-call(bf16[512,2048]{1,0:T(8,128)(2,1)} %tokens_h.1, bf16[1024,2048]{1,0:T(8,128)(2,1)} %bitcast.7, s32[4,8]{1,0:T(4,128)} %bitcast.12, f32[1,2048]{1,0:T(1,128)} %bitcast.8, bf16[2048,256]{1,0:T(8,128)(2,1)} %gv_h.1, bf16[2048,256]{1,0:T(8,128)(2,1)} %gg_h.1, bf16[31,256]{1,0:T(8,128)(2,1)} %taps_h.1, ...), custom_call_target="tpu_custom_call" | custom-call | tf_op jit(solution)/shard_map/layer/pallas_call | solution.py:766
  57.4 0.8 %copy.18 = bf16[128,2048]{1,0:T(8,128)(2,1)} copy(bf16[128,2048]{1,0:T(8,128)(2,1)S(1)} %layer.1) | data formatting | bytes 1048576

commit v4 on v3

--- a/solution.py
+++ b/solution.py
@@ -217,6 +217,7 @@
 RC = 512
 SUB = 8
 EARLY = 5
+LATE = 4
 
 
 def mm(a, b):
@@ -323,25 +324,25 @@
 
     quarter = mo2.at[0:n_piece * PR_]
 
-    def relay_near(*pieces):
+    def relay_near(*steps):
         @pl.when(inner)
         def _():
-            for p in pieces:
+            for p in steps:
                 weight_copy(0, p, grp, core).wait_recv()
                 weight_copy(2, p, grp, core).start()
                 weight_copy(1, p, grp, core).start()
 
-    def relay_far(*pieces):
+    def relay_far(*steps):
         @pl.when(inner)
         def _():
-            for p in pieces:
+            for p in steps:
                 weight_copy(2, p, 1 - grp, core).wait_recv()
                 weight_copy(3, p, 1 - grp, core).start()
 
-    def weights_out(*pieces):
+    def weights_out(*steps):
         @pl.when(outer)
         def _():
-            for p in pieces:
+            for p in steps:
                 weight_copy(0, p, grp, core).start()
 
     pl.semaphore_wait(barrier, n_st - 1 + n_tp - 1 + 1)
@@ -377,7 +378,7 @@
             src = q_stage.at[rows] if stage else q_all.at[st, rows]
             yield remote(src, q_all.at[st, rows], q_send, q_recv.at[k], "st", to)
 
-    for k in range(n_tp):
+    for k in range(n_tp - 1):
         for c in q_copies(k):
             c.start()
 
@@ -503,20 +504,30 @@
     def order(i):
         return lax.rem(chip + 1 + i // 2, n_chip) * 2 + lax.rem(core + 1 - i % 2, 2)
 
-    def answer_copies(k, r):
-        rows = chunk_ds(chunks[k])
+    pieces = [(0, u, u + 1) for u in range(chunk_blocks)] + [(k, 0, chunk_blocks) for k in range(1, n_tp)]
+
+    def piece_rows(n):
+        k, first, last = pieces[n]
+        at = pl.multiple_of(chunks[k] * chunk_rows + first * block_len, block_len)
+        return pl.ds(at, (last - first) * block_len)
+
+    def answer_copies(n, r):
+        rows = piece_rows(n)
         return (
-            remote(out_o.at[r, rows], ret_o.at[st, rows], o_send, o_recv.at[k], "st", r),
-            remote(out_s.at[r, k], ret_s.at[st, k], s_send, s_recv.at[k], "st", r),
+            remote(out_o.at[r, rows], ret_o.at[st, rows], o_send, o_recv.at[n], "st", r),
+            remote(out_s.at[r, n], ret_s.at[st, n], s_send, s_recv.at[n], "st", r),
         )
 
-    def attend(k):
+    def attend(m):
+        k, first, last = pieces[m]
         d = chunks[k]
         rows = chunk_ds(d)
+        spare = jnp.zeros((chunk_rows - (last - first) * block_len, 1), F32)
 
         rs = [order(i) for i in range(n_st)]
-        drain(q_all.at[0:n_st - 1, rows], q_recv.at[k])
-        units = [(e, h, u) for e in range(n_st) for h in range(heads) for u in range(chunk_blocks)]
+        if first == 0:
+            drain(q_all.at[0:n_st - 1, rows], q_recv.at[k])
+        units = [(e, h, u) for e in range(n_st) for h in range(heads) for u in range(first, last)]
         place, values, scores, tops, dens, weights = {}, {}, {}, {}, {}, {}
         for e, h, u in units:
             r = rs[e]
@@ -552,26 +563,28 @@
             for e in range(2):
                 for h in range(heads):
                     for at, parts in ((2 * h, tops), (2 * h + 1, dens)):
-                        column = jnp.concatenate([parts[e0 + e, h, u] for u in range(chunk_blocks)], axis=0)
+                        column = [parts[e0 + e, h, u] for u in range(first, last)]
+                        column = jnp.concatenate(column + [spare] * (spare.shape[0] > 0), axis=0)
                         stats = jnp.where(clane == 8 * e + at, column, stats)
             turned = jnp.transpose(stats)
             for e in range(2):
                 r = rs[e0 + e]
-                out_s[r, k] = turned[8 * e:8 * e + 8]
+                out_s[r, m] = turned[8 * e:8 * e + 8]
                 if e0 + e < n_st - 1:
-                    for c in answer_copies(k, r):
+                    for c in answer_copies(m, r):
                         c.start()
 
-    attend(0)
+    halves = chunk_blocks
+    for m in range(halves):
+        attend(m)
+    for c in q_copies(n_tp - 1):
+        c.start()
     relay_near(2)
     conv_pair(1)
     relay_near(3)
     relay_far(0)
-    attend(1)
+    attend(halves)
     relay_far(1)
-    attend(2)
-    relay_near(4)
-    relay_far(2)
     smalls[5].wait()
     smalls[6].wait()
     act_pair(0)
@@ -579,7 +592,7 @@
     loads[8].wait()
 
     SR = chunk_rows // SUB
-    AH = chunk_rows // 2
+    cuts = {1: (0, 2 * SR, 4 * SR, chunk_rows), 2: (0, chunk_rows // 2, chunk_rows)}
     NC = 512
 
     def piece(lane, u):
@@ -590,21 +603,32 @@
         box = inbox.at[slot, pl.ds(u * SR, SR)]
         return rows, slot, remote(part.at[rows], box, r_send, r_recv.at[slot, u], "tp", to)
 
-    def rows_copies(k, half):
-        rows = pl.ds(pl.multiple_of(chunks[k] * chunk_rows + half * AH, AH), AH)
-        cut = pl.ds(half * AH, AH)
+    def rows_copies(k, n):
+        at, size = cuts[k][n], cuts[k][n + 1] - cuts[k][n]
+        rows = pl.ds(pl.multiple_of(chunks[k] * chunk_rows + at, 2 * SR), size)
+        cut = pl.ds(at, size)
         return (
-            remote(act.at[rows], mate_act.at[k - 1, cut], a_send.at[0], a_recv.at[0, k - 1, half], "tp", mate),
-            remote(att.at[k, cut], mate_att.at[k - 1, cut], a_send.at[1], a_recv.at[1, k - 1, half], "tp", mate),
+            remote(act.at[rows], mate_act.at[k - 1, cut], a_send.at[0], a_recv.at[0, k - 1, n], "tp", mate),
+            remote(att.at[k, cut], mate_att.at[k - 1, cut], a_send.at[1], a_recv.at[1, k - 1, n], "tp", mate),
         )
 
-    def combine(k):
-        rows = chunk_ds(chunks[k])
-        drain(ret_o.at[0:n_st - 1, rows], o_recv.at[k])
-        drain(ret_s.at[0:n_st - 1, k], s_recv.at[k])
-        ret_s[st, k] = out_s[st, k]
+    def rows_out(k):
+        @pl.when(outer)
+        def _():
+            for n in range(len(cuts[k]) - 1):
+                for c in rows_copies(k, n):
+                    c.start()
+
+    def combine(m):
+        k, first, last = pieces[m]
+        rows = piece_rows(m)
+        cut = slice(first * block_len, last * block_len)
+        drain(ret_o.at[0:n_st - 1, rows], o_recv.at[m])
+        drain(ret_s.at[0:n_st - 1, m], s_recv.at[m])
+        ret_s[st, m] = out_s[st, m]
         stats = jnp.transpose(jnp.concatenate(
-            [ret_s[c, k] for c in range(n_st)] + [jnp.zeros((128 - 8 * n_st, chunk_rows), F32)], axis=0))
+            [ret_s[c, m] for c in range(n_st)] + [jnp.zeros((128 - 8 * n_st, chunk_rows), F32)], axis=0))
+        stats = stats[:(last - first) * block_len]
         ret_o[st, rows, :] = out_o[st, rows, :]
         for g in range(2):
             for h in range(heads):
@@ -616,98 +640,118 @@
                     w = jnp.exp(stats[:, at[c]:at[c] + 1] - best)
                     num = num + w * ret_o[c * 2 + g, rows, cols].astype(F32)
                     den = den + w * stats[:, at[c] + 1:at[c] + 2]
-                att[k, :, (g * heads + h) * HD_:(g * heads + h + 1) * HD_] = (num / den).astype(BF)
-
-    def own_partial(k):
-        rows = chunk_ds(chunks[k])
+                att[k, cut, (g * heads + h) * HD_:(g * heads + h + 1) * HD_] = (num / den).astype(BF)
+
+    def own_partial(m):
+        k, first, last = pieces[m]
+        rows = piece_rows(m)
+        cut = slice(first * block_len, last * block_len)
         for i in range(part.shape[1] // NC):
             cols = slice(i * NC, (i + 1) * NC)
-            part[rows, cols] = (mm(act[rows, :], mo[:, cols]) + blend_gain[:, cols] * mm(att[k], ao[:, cols])).astype(BF)
-
-    def mate_rows(slot, half, cols):
-        cut = slice(half * AH, (half + 1) * AH)
-        return (mm(mate_act[slot, cut], mo2[:, cols])
-                + blend_gain[:, cols] * mm(mate_att[slot, cut], ao2[:, cols])).astype(BF)
-
-    def wait_rows(k, half):
-        for c in rows_copies(k, half):
+            part[rows, cols] = (mm(act[rows, :], mo[:, cols]) + blend_gain[:, cols] * mm(att[k, cut], ao[:, cols])).astype(BF)
+
+    def mate_rows(k, n):
+        for c in rows_copies(k, n):
             c.wait_recv()
-
-    def onward(lane_in, lane_out, *pieces):
-        for u in pieces:
+        cut = slice(cuts[k][n], cuts[k][n + 1])
+        rows = pl.ds(pl.multiple_of(chunks[k] * chunk_rows + cuts[k][n], 2 * SR), cuts[k][n + 1] - cuts[k][n])
+        for i in range(part.shape[1] // NC):
+            cols = slice(i * NC, (i + 1) * NC)
+            value = (mm(mate_act[k - 1, cut], mo2[:, cols])
+                     + blend_gain[:, cols] * mm(mate_att[k - 1, cut], ao2[:, cols])).astype(BF)
+            if k == 1:
+                part[rows, cols] = (part[rows, cols].astype(F32) + value.astype(F32)).astype(BF)
+            else:
+                mate_part[cut, cols] = value
+
+    def send(lane, *steps):
+        for u in steps:
+            piece(lane, u)[2].start()
+
+    def onward(lane_in, lane_out, *steps):
+        for u in steps:
             slot = (0, 1, 2, 0)[lane_in]
             piece(lane_in, u)[2].wait_recv()
             rows, _, copy = piece(lane_out, u)
             part[rows, :] = (part[rows, :].astype(F32) + inbox[slot, pl.ds(u * SR, SR), :].astype(F32)).astype(BF)
             copy.start()
 
-    combine(0)
-    own_partial(0)
+    for m in range(halves):
+        combine(m)
+        own_partial(m)
+
+        @pl.when(outer)
+        def _(m=m):
+            for u in range(m * SUB // halves, min((m + 1) * SUB // halves, EARLY)):
+                piece(0, u)[2].start()
+
+    relay_near(4)
+    relay_far(2)
+    attend(halves + 1)
+    relay_near(5)
+    act_pair(1)
+    relay_far(3)
+
+    @pl.when(inner)
+    def _():
+        onward(0, 1, 0)
+
+    combine(halves)
+    rows_out(1)
 
     @pl.when(outer)
     def _():
-        for u in range(EARLY):
-            piece(0, u)[2].start()
-
-    relay_near(5)
-    relay_far(3)
-    act_pair(1)
-    attend(3)
-    combine(1)
-
-    @pl.when(outer)
-    def _():
-        for half in range(2):
-            for c in rows_copies(1, half):
-                c.start()
-        for u in range(EARLY, SUB):
-            piece(0, u)[2].start()
+        send(0, *range(EARLY, SUB))
 
     @pl.when(inner)
     def _():
-        onward(0, 1, 0)
-        own_partial(1)
+        own_partial(halves)
         onward(0, 1, 1)
 
-    combine(2)
-
-    @pl.when(outer)
-    def _():
-        for half in range(2):
-            for c in rows_copies(2, half):
-                c.start()
-
-    relay_far(4, 5)
+    attend(halves + 2)
 
     @pl.when(inner)
     def _():
-        onward(0, 1, *range(2, EARLY))
-        own_partial(2)
-
-    combine(3)
-    own_partial(3)
+        onward(0, 1, 2)
+
+    combine(halves + 1)
+    rows_out(2)
+    relay_far(4)
+
+    @pl.when(inner)
+    def _():
+        onward(0, 1, 3)
+        own_partial(halves + 1)
+        onward(0, 1, *range(4, EARLY))
+
+    relay_far(5)
 
     @pl.when(inner)
     def _():
         for n in range(2):
             drain(quarter, pass_recv.at[n])
-        for half in range(2):
-            wait_rows(1, half)
-            rows = pl.ds(pl.multiple_of(chunks[1] * chunk_rows + half * AH, AH), AH)
-            for i in range(part.shape[1] // NC):
-                cols = slice(i * NC, (i + 1) * NC)
-                part[rows, cols] = (part[rows, cols].astype(F32) + mate_rows(0, half, cols).astype(F32)).astype(BF)
-            for u in range(half * SUB // 2, (half + 1) * SUB // 2):
-                piece(2, u)[2].start()
-            if half == 0:
-                onward(0, 1, *range(EARLY, SUB))
-        onward(1, 3, *range(EARLY))
-        for half in range(2):
-            wait_rows(2, half)
-            for i in range(part.shape[1] // NC):
-                cols = slice(i * NC, (i + 1) * NC)
-                mate_part[half * AH:(half + 1) * AH, cols] = mate_rows(1, half, cols)
-        onward(1, 3, *range(EARLY, SUB))
+        mate_rows(1, 0)
+        send(2, 0, 1)
+        mate_rows(1, 1)
+        send(2, 2, 3)
+        onward(1, 3, 0, 1)
+        mate_rows(1, 2)
+
+    combine(halves + 2)
+    own_partial(halves + 2)
+
+    @pl.when(inner)
+    def _():
+        send(2, *range(4, LATE))
+        onward(1, 3, 2, 3)
+        onward(0, 1, 5, 6)
+        onward(1, 3, 4)
+        onward(0, 1, 7)
+        send(2, *range(LATE, SUB))
+        mate_rows(2, 0)
+        onward(1, 3, 5)
+        mate_rows(2, 1)
+        onward(1, 3, 6, 7)
         for u in range(SUB):
             rows = pl.ds(pl.multiple_of(tp * chunk_rows + u * SR, SR), SR)
             cut = pl.ds(u * SR, SR)
@@ -759,6 +803,7 @@
     nb, per_block = passage_ids.shape
     pad = 8 * pl.cdiv((conv_taps.shape[0] - 1) // 2, 8)
     DMA = pltpu.SemaphoreType.DMA
+    n_ans = n_tp - 1 + nb // n_tp
     V = pltpu.VMEM
     kern = functools.partial(layer_kernel, n_st, n_tp, nb, per_block, T // nb, W // HD, SEQ_LEN, PR)
     hbm = pl.BlockSpec(memory_space=pl.ANY)
@@ -780,12 +825,12 @@
             DMA, DMA((2,)),
             V((T // SEQ_LEN, SEQ_LEN + 2 * pad, CL), F32), V((T, CL), F32), V((T, 128), F32),
             V((n_tp, 2, 8, 2 * T // n_tp), F32), DMA, DMA((2,)), V((T, CL), BF),
-            V((n_st, T, HW), BF), V((n_st, n_tp, 8, T // n_tp), F32), V((n_st, T, HW), BF),
-            V((n_st, n_tp, 8, T // n_tp), F32),
-            DMA, DMA((n_tp,)), DMA, DMA((n_tp,)),
+            V((n_st, T, HW), BF), V((n_st, n_ans, 8, T // n_tp), F32), V((n_st, T, HW), BF),
+            V((n_st, n_ans, 8, T // n_tp), F32),
+            DMA, DMA((n_ans,)), DMA, DMA((n_ans,)),
             V((T, D), BF), V((3, T // n_tp, D), BF), DMA, DMA((3, SUB)),
             V((n_tp, T // n_tp, W), BF), V((2, T // n_tp, CL), BF), V((2, T // n_tp, W), BF),
-            DMA((2,)), DMA((2, 2, 2)), V((T // n_tp, D), BF), V((CL, D), BF), V((W, D), BF),
+            DMA((2,)), DMA((2, 2, 3)), V((T // n_tp, D), BF), V((CL, D), BF), V((W, D), BF),
             DMA((4,)), DMA(((W + CL) // 128,)), DMA(((W + CL) // 128,)), DMA((2,)),
         ],
         compiler_params=pltpu.CompilerParams(
@@ -821,7 +866,7 @@
     def body(*args):
         even = args[11].shape[1] // HD % 2 == 0 and mesh.shape["st"] % 2 == 0
         even = even and args[2].shape[0] % mesh.shape["tp"] == 0 and mesh.shape["st"] <= 16
-        even = even and mesh.shape["tp"] == 4 and mesh.shape["grp"] == 2 and mesh.shape["st"] == 4
+        even = even and mesh.shape["tp"] == 4 and mesh.shape["grp"] == 2 and mesh.shape["st"] == 4 and args[2].shape[0] // mesh.shape["tp"] == 2
         even = even and args[0].shape[0] % (SEQ_LEN * mesh.shape["tp"]) == 0
         return (fused_local if even else local)(*args)
 

time: 58.3 us -> 52.7 us (0.904)
  Pallas kernels: 57.4 us -> 51.7 us
    pallas_call x1, Pallas kernels: 57.4 us -> 51.7 us  [fused_local(): pl.pallas_call(kern, out_shape=pltpu.VMEM((T // n_tp, D), BF), in_specs=[...]
where the time goes in v4:
time: 52.7 us; the launch traced here: 52.5 us
  Pallas kernels  51.7 us (98%)
  local copies, waits for them, and re-layouts  0.8 us (2%)
    pallas_call x1, Pallas kernels, fused_local(): pl.pallas_call(kern, out_shape=pltpu.VMEM((T // n_tp, D), BF), in_specs=[...  51.7 us

profile of v4, /device:TPU:0, one launch (start us, length us, event | category | flops | bytes accessed | tf_op | source)
XLA Modules:
  0.0 52.5 jit_solution(16360696149805496898)
XLA Ops:
  0.0 51.7 %layer.1 = bf16[128,2048]{1,0:T(8,128)(2,1)S(1)} custom-call(bf16[512,2048]{1,0:T(8,128)(2,1)} %tokens_h.1, bf16[1024,2048]{1,0:T(8,128)(2,1)} %bitcast.7, s32[4,8]{1,0:T(4,128)} %bitcast.12, f32[1,2048]{1,0:T(1,128)} %bitcast.8, bf16[2048,256]{1,0:T(8,128)(2,1)} %gv_h.1, bf16[2048,256]{1,0:T(8,128)(2,1)} %gg_h.1, bf16[31,256]{1,0:T(8,128)(2,1)} %taps_h.1, ...), custom_call_target="tpu_custom_call" | custom-call | tf_op jit(solution)/shard_map/layer/pallas_call | solution.py:811
  51.7 0.8 %copy.18 = bf16[128,2048]{1,0:T(8,128)(2,1)} copy(bf16[128,2048]{1,0:T(8,128)(2,1)S(1)} %layer.1) | data formatting | bytes 1048576
